TPU v7x, 512 devices: a whole 4x4x16 slice. The times are simulated.
512 devices in a mesh: ep: 128 (over z, x, core), tp: 4 (over y).
Axes of the slice: x: 4, y: 4, z: 16, core: 2. Of those that a mesh axis runs over, the one named last changes fastest.
Arguments:
- hidden_in: bfloat16 [2048, 1024], P('ep', 'tp'), may hold values from -40 to 40
- norm_gain_attn: float32 [1024], replicated, may hold values from 0.1 to 1.9
- query_weight: bfloat16 [1024, 512], P(None, 'tp'), may hold values from -0.1875 to 0.1875
- key_weight: bfloat16 [1024, 512], P(None, 'tp'), may hold values from -0.1875 to 0.1875
- value_weight: bfloat16 [1024, 512], P(None, 'tp'), may hold values from -0.1875 to 0.1875
- query_gain: float32 [128], replicated, may hold values from 1 to 1.6
- key_gain: float32 [128], replicated, may hold values from 1 to 1.6
- lambda_head: float32 [4], P('tp'), may hold values from 0.3 to 0.8
- sub_gain: float32 [128], replicated, may hold values from 0.1 to 1.9
- out_weight: bfloat16 [512, 1024], P('tp'), may hold values from -0.25 to 0.25
- cache_key: bfloat16 [2048, 256, 512], P('ep', None, 'tp'), may hold values from -8 to 8
- cache_value: bfloat16 [2048, 256, 512], P('ep', None, 'tp'), may hold values from -6 to 6
- lengths: int32 [2048], P('ep'), may hold values from 1 to 256
- norm_gain_mix: float32 [1024], P('tp'), may hold values from 0.1 to 1.9
- route_ids: int32 [2048, 6], P('ep'), may hold values from 0 to 127, all different within a row; in each aligned block of 16 rows (0 to 15, 16 to 31, ...) at most 2 rows name the same one
- route_logits: float32 [2048, 6], P('ep'), may hold values from -4 to 4
- expert_gate: bfloat16 [128, 1024, 1024], P('ep', None, 'tp'), may hold values from -0.5 to 0.5
- expert_up: bfloat16 [128, 1024, 1024], P('ep', None, 'tp'), may hold values from -0.5 to 0.5
- expert_down: bfloat16 [128, 1024, 1024], P('ep', 'tp'), may hold values from -0.046875 to 0.046875
- dense_gate: bfloat16 [1024, 2048], P('tp', 'ep'), may hold values from -0.1875 to 0.1875
- dense_up: bfloat16 [1024, 2048], P('tp', 'ep'), may hold values from -0.1875 to 0.1875
- dense_down: bfloat16 [2048, 1024], P('ep', 'tp'), may hold values from -0.125 to 0.125
- branch_gate: float32 [1024], P('tp'), may hold values from -0.1875 to 0.1875
Outputs:
- layer_out: bfloat16 [2048, 1024], P('ep', 'tp')
- key_rows: bfloat16 [2048, 512], P('ep', 'tp')
- value_rows: bfloat16 [2048, 512], P('ep', 'tp')
Inputs may be any that keep to these rules, and one draw needn't show every extreme that they name: `route_ids`: each row names 6 different experts. Among the rows of one index of ep (aligned blocks of 16 rows) no expert is named by more than 2 rows, and in some blocks one expert is named by exactly 2.
All inputs are finite; a program needn't handle non-finite values.
Results may differ from a plain program's by a relative error of at most 0.0075.
Values may be sent and summed in bfloat16 or wider, within the bound.
No kernel may reach another device: no remote copies, remote signals or barrier semaphores. Data moves between devices by JAX's collectives and lax.ppermute only.
A program may use at most 64 MiB of HBM per device.

v0:
```python
import math

import jax
import jax.numpy as jnp
from jax import lax
from jax.experimental import pallas as pl
from jax.experimental.pallas import tpu as pltpu

from jax.sharding import Mesh
from jax.sharding import PartitionSpec as P


EP = ("ep_0", "ep_1", "ep_2")
BLOCK = ("ep_1", "ep_2", "tp")
CAP = 2


EPSILON = 1e-06
CLAMP_LIMIT = 7.0
SWISH_ALPHA = 1.702
OUT_SCALE = 0.2 + 0.6 * math.exp(-0.6)


def clamped_unit(gate_pre, up_pre):
    gate_cut = jnp.minimum(gate_pre, CLAMP_LIMIT)
    up_cut = jnp.clip(up_pre, -CLAMP_LIMIT, CLAMP_LIMIT)
    return (up_cut + 1.0) * gate_cut * jax.nn.sigmoid(SWISH_ALPHA * gate_cut)


LANES = 128
TURNED = (((0,), (0,)), ((), ()))
ACROSS = (((1,), (1,)), ((), ()))
SCALARS = pl.BlockSpec(memory_space=pltpu.SMEM)
LIMIT = pltpu.CompilerParams(vmem_limit_bytes=12 * 2**20)
WHOLE = pl.BlockSpec(memory_space=pltpu.VMEM)


def mm(a, b):
    return jnp.dot(a, b, preferred_element_type=jnp.float32)


def sent_to_hbm(shape, dtype):
    return pltpu.HBM(shape, dtype)


def kept(x):
    return pltpu.VMEM(x.shape, x.dtype)


def far(x):
    return pltpu.with_memory_space_constraint(x, pltpu.HBM)


def near(x):
    return pltpu.with_memory_space_constraint(x, pltpu.VMEM)


def opening_kernel(hidden_ref, gate_ref, up_ref, down_ref, gain_ref, branch_ref, out_ref):
    lean = gain_ref[...] * branch_ref[...]
    high = lean.astype(jnp.bfloat16).astype(jnp.float32)
    row = lax.broadcasted_iota(jnp.int32, (8, lean.shape[1]), 0)
    extra = jnp.where(row == 0, high, jnp.where(row == 1, lean - high, 0.0))
    extra = extra.astype(jnp.bfloat16)
    seq, units = hidden_ref.shape[0], down_ref.shape[0]
    past = seq + 3 * units
    for k in range(out_ref.shape[0]):
        out_ref[k, :seq, :] = hidden_ref[...]
        out_ref[k, seq : seq + units, :] = gate_ref[...]
        out_ref[k, seq + units : seq + 2 * units, :] = up_ref[...]
        out_ref[k, seq + 2 * units : past, :] = down_ref[...]
        out_ref[k, past:, :] = extra


def routes_kernel(ids_ref, turned_ref, logits_ref, out_ref):
    ids = ids_ref[...]
    turned = turned_ref[...]
    count, top = ids.shape
    logits = logits_ref[...]
    grown = jnp.exp(logits - jnp.max(logits, axis=1, keepdims=True))
    weight = grown / jnp.sum(grown, axis=1, keepdims=True)
    upper = weight.astype(jnp.bfloat16).astype(jnp.float32)
    lower = weight - upper
    row = lax.broadcasted_iota(jnp.int32, (count, count), 0)
    col = lax.broadcasted_iota(jnp.int32, (count, count), 1)
    lane = lax.broadcasted_iota(jnp.int32, (count, LANES), 1)
    packed = jnp.zeros((count, LANES), jnp.float32)
    for k in range(top):
        mine = ids[:, k : k + 1]
        same = jnp.zeros((count, count), jnp.float32)
        for other in range(top):
            same = same + jnp.where(mine == turned[other : other + 1, :], 1.0, 0.0)
        rank = jnp.sum(jnp.where(col < row, same, 0.0), axis=1, keepdims=True)
        code = mine.astype(jnp.float32) * CAP + rank
        packed = jnp.where(lane == k, code, packed)
        packed = jnp.where(lane == top + k, upper[:, k : k + 1], packed)
        packed = jnp.where(lane == 2 * top + k, lower[:, k : k + 1], packed)
    out_ref[...] = packed


def stage_kernel(*refs):
    count = len(refs) // 2
    sems = refs[-1]
    moves = [
        pltpu.make_async_copy(refs[k], refs[count + k], sems.at[k]) for k in range(count)
    ]
    for move in moves:
        move.start()
    for move in moves:
        move.wait()


def attend_kernel(
    lambda_ref,
    pieces_ref,
    gain_ref,
    query_ref,
    key_ref,
    value_ref,
    query_gain_ref,
    key_gain_ref,
    sub_ref,
    out_weight_ref,
    past_key_ref,
    past_value_ref,
    lengths_ref,
    out_ref,
    key_rows_ref,
    value_rows_ref,
):
    seq, past, size = past_key_ref.shape
    tp = pieces_ref.shape[0]
    half = size // 2
    full = jnp.concatenate([pieces_ref[k, :seq, :] for k in range(tp)], axis=1)
    full = full.astype(jnp.float32)
    square = jnp.sum(full * full, axis=1, keepdims=True) / full.shape[1]
    normed = (full * lax.rsqrt(square + EPSILON) * gain_ref[...]).astype(jnp.bfloat16)
    first = lax.broadcasted_iota(jnp.int32, (seq, size), 1) < half

    def halves(x):
        return (
            jnp.sum(jnp.where(first, x, 0.0), axis=1, keepdims=True),
            jnp.sum(jnp.where(first, 0.0, x), axis=1, keepdims=True),
        )

    def scaled(x, gain):
        low, high = halves(x * x)
        inverse = jnp.where(
            first, lax.rsqrt(low / half + EPSILON), lax.rsqrt(high / half + EPSILON)
        )
        return (x * inverse * gain).astype(jnp.bfloat16)

    query = scaled(mm(normed, query_ref[...]), query_gain_ref[...])
    key = scaled(mm(normed, key_ref[...]), key_gain_ref[...])
    value = mm(normed, value_ref[...]).astype(jnp.bfloat16)
    key_rows_ref[...] = key
    value_rows_ref[...] = value
    query = query.astype(jnp.float32)
    both = jnp.concatenate(
        [jnp.where(first, query, 0.0), jnp.where(first, 0.0, query)], axis=0
    )
    row = lax.broadcasted_iota(jnp.int32, (2 * seq, size), 0) % seq
    score = jnp.zeros((2 * seq, past), jnp.float32)
    for k in range(seq):
        mine = jnp.where(row == k, both, 0.0).astype(jnp.bfloat16)
        score = score + lax.dot_general(
            mine, past_key_ref[k], ACROSS, preferred_element_type=jnp.float32
        )
    scale = half**-0.5
    valid = lax.broadcasted_iota(jnp.int32, (seq, past), 1) < lengths_ref[...]
    own = [jnp.exp(o * scale) for o in halves(query * key.astype(jnp.float32))]
    grown = [
        jnp.where(valid, jnp.exp(score[m * seq : (m + 1) * seq] * scale), 0.0) for m in range(2)
    ]
    total = [jnp.sum(g, axis=1, keepdims=True) + o for g, o in zip(grown, own)]
    share = lambda_ref[0]
    weight = (grown[0] / total[0] - share * (grown[1] / total[1])).astype(jnp.bfloat16)
    weight_own = (own[0] / total[0] - share * (own[1] / total[1])).astype(jnp.bfloat16)
    weight = weight.astype(jnp.float32)
    row = lax.broadcasted_iota(jnp.int32, (seq, past), 0)
    mixed = weight_own.astype(jnp.float32) * value.astype(jnp.float32)
    for k in range(seq):
        mine = jnp.where(row == k, weight, 0.0).astype(jnp.bfloat16)
        mixed = mixed + mm(mine, past_value_ref[k])
    square = jnp.sum(mixed * mixed, axis=1, keepdims=True) / size
    head = mixed * lax.rsqrt(square + EPSILON) * sub_ref[...] * OUT_SCALE
    part = mm(head.astype(jnp.bfloat16), out_weight_ref[...]).astype(jnp.bfloat16)
    for k in range(tp):
        out_ref[k] = part


def mix_kernel(tp_ref, parts_ref, pieces_ref, gain_ref, routes_ref, res_ref, out_ref, *, top):
    tp, seq, _ = parts_ref.shape
    past = pieces_ref.shape[1] - 8
    residual = jnp.concatenate([pieces_ref[k, :seq, :] for k in range(tp)], axis=1)
    residual = residual.astype(jnp.float32)
    for k in range(tp):
        residual = residual + parts_ref[k].astype(jnp.float32)
    ends = [pieces_ref[k, past:, :].astype(jnp.float32) for k in range(tp)]
    lean = jnp.concatenate([end[0:1] + end[1:2] for end in ends], axis=1)
    total = residual.shape[1]
    width = total // tp
    inverse = lax.rsqrt(jnp.sum(residual * residual, axis=1, keepdims=True) / total + EPSILON)
    logit = jnp.sum(residual * lean, axis=1, keepdims=True) * inverse
    branch = jax.nn.sigmoid(logit)
    upper = branch.astype(jnp.bfloat16).astype(jnp.float32)
    own = jnp.zeros((residual.shape[0], width), jnp.float32)
    for k in range(tp):
        own = own + jnp.where(tp_ref[0] == k, residual[:, k * width : (k + 1) * width], 0.0)
    res_ref[...] = own
    mix = (own * inverse * gain_ref[...]).astype(jnp.bfloat16)
    routes = routes_ref[...]
    lane = lax.broadcasted_iota(jnp.int32, routes.shape, 1)
    routes = jnp.where(lane == 3 * top, upper, routes)
    routes = jnp.where(lane == 3 * top + 1, branch - upper, routes)
    rows = out_ref.shape[1] - width // LANES * seq
    stride = LANES * rows // seq
    notes = routes[:rows]
    for g in range(1, seq // rows):
        notes = notes + pltpu.roll(routes[g * rows : (g + 1) * rows], stride * g, axis=1)
    notes = notes.astype(jnp.bfloat16)
    for k in range(out_ref.shape[0]):
        for h in range(width // LANES):
            out_ref[k, h * seq : (h + 1) * seq, :] = mix[:, h * LANES : (h + 1) * LANES]
        out_ref[k, width // LANES * seq :, :] = notes


def notes_of(seen_ref, seq):
    line = seen_ref.shape[0]
    rows = seen_ref.shape[1] % seq
    packed = seen_ref[:, seen_ref.shape[1] - rows :, :].astype(jnp.float32)
    stride = LANES * rows // seq
    turned = [packed]
    for g in range(1, seq // rows):
        turned.append(pltpu.roll(packed, LANES - stride * g, axis=2))
    return jnp.concatenate(turned, axis=1).reshape(line * seq, LANES)


def slot_hits(notes, first, line, plane, top):
    total = notes.shape[0]
    slots = plane * line * CAP
    row = lax.broadcasted_iota(jnp.int32, (total, slots), 0)
    col = lax.broadcasted_iota(jnp.int32, (total, slots), 1)
    code = (first + col // (line * CAP)) * CAP + col % CAP
    here = row // (total // line) == (col // CAP) % line
    code = jnp.where(here, code, -1).astype(jnp.float32)
    return [notes[:, k : k + 1] == code for k in range(top)]


def outward_kernel(first_ref, seen_ref, out_hbm, placed_ref, dealt_ref, sems, *, top, seq):
    line = seen_ref.shape[0]
    plane, tp, items, width = out_hbm.shape
    slots = line * CAP
    rows = jnp.concatenate(
        [
            seen_ref[:, h * seq : (h + 1) * seq, :].reshape(line * seq, LANES)
            for h in range(width // LANES)
        ],
        axis=1,
    )
    dealt = rows.astype(jnp.float32).reshape(plane, tp, items - slots, width)
    dealt_ref[...] = dealt.astype(jnp.bfloat16)
    moves = [
        pltpu.make_async_copy(dealt_ref, out_hbm.at[:, :, pl.ds(slots, items - slots)], sems.at[tp])
    ]
    moves[0].start()
    hits = slot_hits(notes_of(seen_ref, seq), first_ref[0], line, plane, top)
    select = sum(jnp.where(h, 1.0, 0.0) for h in hits).astype(jnp.bfloat16)
    placed = lax.dot_general(select, rows, TURNED, preferred_element_type=jnp.float32)
    placed_ref[...] = placed.astype(jnp.bfloat16).reshape(plane, slots, width)
    for k in range(tp):
        moves.append(
            pltpu.make_async_copy(placed_ref, out_hbm.at[:, k, pl.ds(0, slots)], sems.at[k])
        )
        moves[-1].start()
    for move in moves:
        move.wait()


def weights_kernel(first_ref, seen_ref, upper_ref, lower_ref, branch_ref, *, top, plane, seq):
    line = seen_ref.shape[0]
    notes = notes_of(seen_ref, seq)
    hits = slot_hits(notes, first_ref[0], line, plane, top)
    upper_ref[...] = sum(
        jnp.where(h, notes[:, top + k : top + k + 1], 0.0) for k, h in enumerate(hits)
    ).astype(jnp.bfloat16)
    lower_ref[...] = sum(
        jnp.where(h, notes[:, 2 * top + k : 2 * top + k + 1], 0.0) for k, h in enumerate(hits)
    ).astype(jnp.bfloat16)
    branch = notes[:, 3 * top : 3 * top + 1] + notes[:, 3 * top + 1 : 3 * top + 2]
    branch_ref[...] = jnp.broadcast_to(branch, branch_ref.shape)


def expert_kernel(
    seen_ref, gate_ref, up_ref, down_hbm, own_hbm, other_hbm, out_hbm, down_ref, dense_ref, out_ref, sems, *, slots
):
    fetches = [
        pltpu.make_async_copy(own_hbm, dense_ref.at[0], sems.at[0]),
        pltpu.make_async_copy(other_hbm, dense_ref.at[1], sems.at[1]),
        pltpu.make_async_copy(down_hbm, down_ref, sems.at[2]),
    ]
    for fetch in fetches:
        fetch.start()
    plane, tp, items, width = seen_ref.shape
    gate_pre = up_pre = 0.0
    for k in range(tp):
        rows = seen_ref[:, k, :slots, :].reshape(plane * slots, width)
        gate_pre = gate_pre + mm(rows, gate_ref[0, k * width : (k + 1) * width, :])
        up_pre = up_pre + mm(rows, up_ref[0, k * width : (k + 1) * width, :])
    act = clamped_unit(gate_pre, up_pre).astype(jnp.bfloat16)
    _, columns, _, rows_each, _ = dense_ref.shape
    units = rows_each // 3
    every = 2 * columns * units
    dealt = items - slots
    fetches[0].wait()
    fetches[1].wait()
    gate_pre = up_pre = 0.0
    for k in range(tp):
        rows = seen_ref[:, k, slots:, :].astype(jnp.float32).reshape(plane * dealt, width)
        rows = rows.astype(jnp.bfloat16)
        gate = dense_ref[:, :, k, :units, :].reshape(every, width)
        up = dense_ref[:, :, k, units : 2 * units, :].reshape(every, width)
        gate_pre = gate_pre + lax.dot_general(
            rows, gate, ACROSS, preferred_element_type=jnp.float32
        )
        up_pre = up_pre + lax.dot_general(rows, up, ACROSS, preferred_element_type=jnp.float32)
    dense_act = (gate_pre / (1.0 + jnp.exp(-gate_pre)) * up_pre).astype(jnp.bfloat16)
    fetches[2].wait()
    moves = []
    for k in range(tp):
        part = mm(act, down_ref[0, :, k * width : (k + 1) * width]).astype(jnp.bfloat16)
        out_ref[k, :, :slots, :] = part.reshape(plane, slots, width)
        down = dense_ref[:, :, k, 2 * units :, :].reshape(every, width)
        part = mm(dense_act, down).reshape(plane, dealt, width)
        out_ref[k, :, slots:, :] = part.astype(jnp.bfloat16)
        moves.append(pltpu.make_async_copy(out_ref.at[k], out_hbm.at[:, k], sems.at[3 + k]))
        moves[-1].start()
    for move in moves:
        move.wait()


def inward_kernel(seen_ref, upper_ref, lower_ref, branch_ref, out_ref):
    line, seq, width = out_ref.shape
    plane, tp, _, _ = seen_ref.shape
    slots = line * CAP
    whole = jnp.zeros((plane, slots, width), jnp.float32)
    for k in range(tp):
        whole = whole + seen_ref[:, k, :slots, :].astype(jnp.float32)
    whole = whole.astype(jnp.bfloat16).reshape(plane * slots, width)
    routed = mm(upper_ref[...], whole) + mm(lower_ref[...], whole)
    dense = seen_ref[:, :, slots:, :].astype(jnp.float32).reshape(line * seq, width)
    back = (routed + branch_ref[...] * dense).astype(jnp.bfloat16)
    out_ref[...] = back.reshape(line, seq, width)


def doubled(held, step):
    columns = lax.axis_size("ep_1")
    other = lax.ppermute(held, "ep_1", [(i, i ^ step) for i in range(columns)])
    return jnp.concatenate([held, other], axis=0)


def shaped(shape, dtype):
    return jax.ShapeDtypeStruct(shape, dtype)


def body(
    hidden_in,
    norm_gain_attn,
    query_weight,
    key_weight,
    value_weight,
    query_gain,
    key_gain,
    lambda_head,
    sub_gain,
    out_weight,
    cache_key,
    cache_value,
    lengths,
    norm_gain_mix,
    route_ids,
    route_logits,
    expert_gate,
    expert_up,
    expert_down,
    dense_gate,
    dense_up,
    dense_down,
    branch_gate,
):
    seq, top = route_ids.shape
    width = hidden_in.shape[1]
    units = dense_down.shape[0]
    line = lax.axis_size("ep_0")
    plane = lax.axis_size("ep_1") * lax.axis_size("ep_2")
    tp = lax.axis_size("tp")
    slots = line * CAP
    dealt = line * seq // (plane * tp)
    past = seq + 3 * units
    mine = pl.pallas_call(
        opening_kernel, out_shape=shaped((tp, past + 8, width), jnp.bfloat16), name="opening", compiler_params=LIMIT
    )(
        *map(
            far,
            (
                hidden_in,
                dense_gate.T,
                dense_up.T,
                dense_down,
                norm_gain_mix[None, :],
                branch_gate[None, :],
            ),
        )
    )
    pieces = lax.all_to_all(mine, "tp", 0, 0, tiled=True)
    needed = (
        norm_gain_attn[None, :],
        query_weight,
        key_weight,
        value_weight,
        query_gain[None, :],
        key_gain[None, :],
        sub_gain[None, :],
        out_weight,
        cache_key,
        cache_value,
        norm_gain_mix[None, :],
    )
    *staged, gain_here = pl.pallas_call(
        stage_kernel,
        out_shape=tuple(map(kept, needed)),
        in_specs=[pl.BlockSpec(memory_space=pl.ANY)] * len(needed),
        out_specs=(WHOLE,) * len(needed),
        scratch_shapes=[pltpu.SemaphoreType.DMA((len(needed),))],
        name="stage",
        compiler_params=LIMIT,
    )(*map(far, needed))
    routes = pl.pallas_call(
        routes_kernel, out_shape=shaped((seq, LANES), jnp.float32), name="routes", compiler_params=LIMIT
    )(route_ids, route_ids.T, route_logits)
    size = value_weight.shape[1]
    parts, key_rows, value_rows = pl.pallas_call(
        attend_kernel,
        out_shape=(
            shaped((tp, seq, out_weight.shape[1]), jnp.bfloat16),
            shaped((seq, size), jnp.bfloat16),
            shaped((seq, size), jnp.bfloat16),
        ),
        in_specs=[SCALARS] + [WHOLE] * 12,
        name="attend",
        compiler_params=LIMIT,
    )(
        lambda_head,
        near(pieces),
        *map(near, staged),
        near(lengths[:, None]),
    )
    parts = lax.all_to_all(parts, "tp", 0, 0, tiled=True)
    columns = lax.axis_size("ep_1")
    steps = [1 << k for k in reversed(range(columns.bit_length() - 1))]
    own_dense = pieces[None, :, seq:past]
    for step in steps[:1]:
        own_dense = doubled(own_dense, step)
    residual, message = pl.pallas_call(
        lambda *refs: mix_kernel(*refs, top=top),
        out_shape=(
            shaped((seq, width), jnp.float32),
            shaped((line, width // LANES * seq + 8, LANES), jnp.bfloat16),
        ),
        in_specs=[SCALARS] + [WHOLE] * 4,
        name="mix",
        compiler_params=LIMIT,
    )(
        lax.axis_index("tp").reshape(1),
        near(parts),
        near(pieces),
        near(gain_here),
        near(routes),
    )
    seen = lax.all_to_all(message, "ep_0", 0, 0, tiled=True)
    for step in steps[1:]:
        own_dense = doubled(own_dense, step)
    own_dense, seen = lax.optimization_barrier((own_dense, seen))
    seen = near(seen)
    other_dense = lax.ppermute(own_dense, "ep_2", [(0, 1), (1, 0)])
    first = (lax.axis_index("ep_0") * plane).reshape(1)
    outward = pl.pallas_call(
        lambda *refs: outward_kernel(*refs, top=top, seq=seq),
        out_shape=sent_to_hbm((plane, tp, slots + dealt, width), jnp.bfloat16),
        in_specs=[SCALARS, WHOLE],
        out_specs=pl.BlockSpec(memory_space=pl.ANY),
        scratch_shapes=[
            pltpu.VMEM((plane, slots, width), jnp.bfloat16),
            pltpu.VMEM((plane, tp, dealt, width), jnp.bfloat16),
            pltpu.SemaphoreType.DMA((tp + 1,)),
        ],
        name="outward",
        compiler_params=LIMIT,
    )(first, seen)
    arrived = lax.all_to_all(
        outward.reshape(plane * tp, slots + dealt, width), BLOCK, 0, 0, tiled=True
    ).reshape(plane, tp, slots + dealt, width)
    upper, lower, branch = pl.pallas_call(
        lambda *refs: weights_kernel(*refs, top=top, plane=plane, seq=seq),
        out_shape=(
            shaped((line * seq, plane * slots), jnp.bfloat16),
            shaped((line * seq, plane * slots), jnp.bfloat16),
            shaped((line * seq, width), jnp.float32),
        ),
        in_specs=[SCALARS, WHOLE],
        name="weights",
        compiler_params=LIMIT,
    )(first, seen)
    sent = pl.pallas_call(
        lambda *refs: expert_kernel(*refs, slots=slots),
        out_shape=sent_to_hbm((plane, tp, slots + dealt, width), jnp.bfloat16),
        in_specs=[WHOLE] * 3 + [pl.BlockSpec(memory_space=pl.ANY)] * 3,
        out_specs=pl.BlockSpec(memory_space=pl.ANY),
        scratch_shapes=[
            pltpu.VMEM(expert_down.shape, expert_down.dtype),
            pltpu.VMEM((2, *own_dense.shape), own_dense.dtype),
            pltpu.VMEM((tp, plane, slots + dealt, width), jnp.bfloat16),
            pltpu.SemaphoreType.DMA((3 + tp,)),
        ],
        name="experts",
        compiler_params=LIMIT,
    )(
        near(arrived),
        near(expert_gate),
        near(expert_up),
        far(expert_down),
        far(own_dense),
        far(other_dense),
    )
    returned = lax.all_to_all(
        sent.reshape(plane * tp, slots + dealt, width), BLOCK, 0, 0, tiled=True
    ).reshape(plane, tp, slots + dealt, width)
    back = pl.pallas_call(
        inward_kernel,
        out_shape=shaped((line, seq, width), jnp.bfloat16),
        name="inward",
        compiler_params=LIMIT,
    )(near(returned), near(upper), near(lower), near(branch))
    home = lax.all_to_all(back, "ep_0", 0, 0, tiled=True)
    layer_out = (residual + jnp.sum(home.astype(jnp.float32), axis=0)).astype(jnp.bfloat16)
    return (layer_out, key_rows, value_rows)


def solution(mesh):
    split = Mesh(mesh.devices.reshape(16, 4, 2, mesh.shape["tp"]), ("ep_0", "ep_1", "ep_2", "tp"))
    in_specs = (
        P(EP, "tp"),
        P(),
        P(None, "tp"),
        P(None, "tp"),
        P(None, "tp"),
        P(),
        P(),
        P("tp"),
        P(),
        P("tp", None),
        P(EP, None, "tp"),
        P(EP, None, "tp"),
        P(EP),
        P("tp"),
        P(EP, None),
        P(EP, None),
        P(EP, None, "tp"),
        P(EP, None, "tp"),
        P(EP, "tp", None),
        P("tp", EP),
        P("tp", EP),
        P(EP, "tp"),
        P("tp"),
    )
    out_specs = (P(EP, "tp"), P(EP, "tp"), P(EP, "tp"))
    return jax.shard_map(body, mesh=split, in_specs=in_specs, out_specs=out_specs, check_vma=False)
```

profile of v0, /device:TPU:32, one launch (start us, length us, event | category | flops | bytes accessed | tf_op | source)
XLA Modules:
  0.0 121.8 jit_solution(10622928603355651674)
XLA Ops:
  0.6 1.4 %opening.1 = bf16[4,72,256]{2,1,0:T(8,128)(2,1)} custom-call(bf16[16,256]{1,0:T(8,128)(2,1)} %hidden_ref.1, bf16[16,256]{1,0:T(8,128)(2,1)} %bitcast.23, bf16[16,256]{1,0:T(8,128)(2,1)} %bitcast.24, bf16[16,256]{1,0:T(8,128)(2,1)} %down_ref.1, f32[1,256]{1,0:T(1,128)} %bitcast.26, f32[1,256]{1,0:T(1,128)} %bitcast.28), custom_call_target="tpu_custom_call" | custom-call | tf_op jit(solution)/shard_map/opening/pallas_call | solution.py:399
  2.1 4.5 %all-to-all-start = ((bf16[4,72,256]{2,1,0:T(8,128)(2,1)}), bf16[4,72,256]{2,1,0:T(8,128)(2,1)S(1)}, u32[]{:S(2)}, u32[]{:S(2)}) async-start(bf16[4,72,256]{2,1,0:T(8,128)(2,1)} %opening.1), calls=%async_computation | async-start | bytes 294912 | tf_op jit(solution)/shard_map/all_to_all | solution.py:414
  7.2 0.0 copy-start.6
  7.2 0.6 copy-done.6
  7.8 0.1 copy.26.lengths_ref
  7.9 2.0 %stage.1 = (f32[1,1024]{1,0:T(1,128)S(1)}, bf16[1024,128]{1,0:T(8,128)(2,1)S(1)}, bf16[1024,128]{1,0:T(8,128)(2,1)S(1)}, bf16[1024,128]{1,0:T(8,128)(2,1)S(1)}, ...) custom-call(f32[1,1024]{1,0:T(1,128)} %bitcast.25, ...), custom_call_target="tpu_custom_call" | custom-call | tf_op jit(solution)/shard_map/stage/pallas_call | solution.py:428
  10.0 2.6 %all-to-all-done.pieces_ref.refs_2_ = bf16[4,72,256]{2,1,0:T(8,128)(2,1)S(1)} async-done(((bf16[4,72,256]{2,1,0:T(8,128)(2,1)}), bf16[4,72,256]{2,1,0:T(8,128)(2,1)S(1)}, u32[]{:S(2)}, u32[]{:S(2)}) %all-to-all-start) | async-done | bytes 147488 | tf_op jit(solution)/shard_map/all_to_all | solution.py:414
  12.6 2.2 %attend.1 = (bf16[4,16,1024]{2,1,0:T(8,128)(2,1)}, bf16[16,128]{1,0:T(8,128)(2,1)}, bf16[16,128]{1,0:T(8,128)(2,1)}) custom-call(f32[1]{0:T(128)S(6)} %copy.29.lambda_ref, bf16[4,72,256]{2,1,0:T(8,128)(2,1)S(1)} %all-to-all-done.pieces_ref.refs_2_, f32[1,1024]{1,0:T(1,128)S(1)} %get-tuple-element.24.gain_ref, ...), custom_call_target="tpu_custom_call" | custom-call | tf_op jit(solution)/shard_map/attend/pallas_call | solution.py:441
  14.8 3.3 %all-to-all-start.1 = ((bf16[4,16,1024]{2,1,0:T(8,128)(2,1)}), bf16[4,16,1024]{2,1,0:T(8,128)(2,1)S(1)}, u32[]{:S(2)}, u32[]{:S(2)}) async-start(bf16[4,16,1024]{2,1,0:T(8,128)(2,1)} %get-tuple-element.34), calls=%async_computation.1 | async-start | bytes 262144 | tf_op jit(solution)/shard_map/all_to_all | solution.py:457
  18.2 0.0 copy-start.2
  18.2 0.7 copy-done.2
  18.9 0.0 copy-start.5
  18.9 0.1 copy.27.ids_ref
  19.0 0.6 copy-done.5
  19.6 0.1 copy.28.logits_ref
  19.6 0.4 routes.1.refs_4_
  20.0 4.1 %all-to-all-done.1.refs_1_ = bf16[4,16,1024]{2,1,0:T(8,128)(2,1)S(1)} async-done(((bf16[4,16,1024]{2,1,0:T(8,128)(2,1)}), bf16[4,16,1024]{2,1,0:T(8,128)(2,1)S(1)}, u32[]{:S(2)}, u32[]{:S(2)}) %all-to-all-start.1) | async-done | bytes 131104 | tf_op jit(solution)/shard_map/all_to_all | solution.py:457
  24.1 0.9 mix.1
  25.0 15.2 %all-to-all-start.2 = ((bf16[16,40,128]{2,1,0:T(8,128)(2,1)}), bf16[16,40,128]{2,1,0:T(8,128)(2,1)S(1)}, u32[]{:S(2)}, u32[]{:S(2)}) async-start(bf16[16,40,128]{2,1,0:T(8,128)(2,1)} %get-tuple-element.37), calls=%async_computation.2 | async-start | bytes 327680 | tf_op jit(solution)/shard_map/all_to_all | solution.py:479
  40.2 4.9 %collective-permute-start = (bf16[1,4,48,256]{3,2,1,0:T(8,128)(2,1)S(1)}, bf16[1,4,48,256]{3,2,1,0:T(8,128)(2,1)S(1)}, u32[]{:S(2)}, u32[]{:S(2)}) collective-permute-start(bf16[1,4,48,256]{3,2,1,0:T(8,128)(2,1)S(1)} %slice_bitcast_fusion), channel_id=1, source_target_pairs={{0,16},{8,24},{16,0},{24,8},{1,17},{9,25},{17,1},{25,9},{2,18},{10... | collective-permute-start | bytes 294920 | tf_op jit(solution)/shard_map/ppermute | solution.py:357
  45.1 3.1 %collective-permute-done = bf16[1,4,48,256]{3,2,1,0:T(8,128)(2,1)S(1)} collective-permute-done((bf16[1,4,48,256]{3,2,1,0:T(8,128)(2,1)S(1)}, bf16[1,4,48,256]{3,2,1,0:T(8,128)(2,1)S(1)}, u32[]{:S(2)}, u32[]{:S(2)}) %collective-permute-start) | collective-permute-done | bytes 98336 | tf_op jit(solution)/shard_map/ppermute | solution.py:357
  48.2 3.4 %collective-permute-start.1 = (bf16[2,4,48,256]{3,2,1,0:T(8,128)(2,1)S(1)}, bf16[2,4,48,256]{3,2,1,0:T(8,128)(2,1)S(1)}, u32[]{:S(2)}, u32[]{:S(2)}) collective-permute-start(bf16[2,4,48,256]{3,2,1,0:T(8,128)(2,1)S(1)} %pad_maximum_fusion.1), channel_id=1, source_target_pairs={{0,8},{8,0},{16,24},{24,16},{1,9},{9,1},{17,25},{25,17},{2,10},{10... | collective-permute-start | bytes 589832 | tf_op jit(solution)/shard_map/ppermute | solution.py:357
  51.7 4.1 %collective-permute-done.1 = bf16[2,4,48,256]{3,2,1,0:T(8,128)(2,1)S(1)} collective-permute-done((bf16[2,4,48,256]{3,2,1,0:T(8,128)(2,1)S(1)}, bf16[2,4,48,256]{3,2,1,0:T(8,128)(2,1)S(1)}, u32[]{:S(2)}, u32[]{:S(2)}) %collective-permute-start.1) | collective-permute-done | bytes 196640 | tf_op jit(solution)/shard_map/ppermute | solution.py:357
  55.8 0.0 copy-start.3
  55.9 0.0 all-to-all-done.2.refs_1_
  55.9 1.4 %outward.1 = bf16[8,4,40,256]{3,2,1,0:T(8,128)(2,1)} custom-call(s32[1]{0:T(128)} %bitcast.11.refs_0_, bf16[16,40,128]{2,1,0:T(8,128)(2,1)S(1)} %all-to-all-done.2.refs_1_), custom_call_target="tpu_custom_call" | custom-call | tf_op jit(solution)/shard_map/outward/pallas_call | solution.py:486
  57.3 0.0 copy-start
  57.3 0.0 copy-start.1
  57.3 5.4 %all-to-all-start.3 = ((bf16[32,40,256]{2,1,0:T(8,128)(2,1)}), bf16[32,40,256]{2,1,0:T(8,128)(2,1)S(1)}, u32[]{:S(2)}, u32[]{:S(2)}) async-start(bf16[32,40,256]{2,1,0:T(8,128)(2,1)} %bitcast.22), calls=%async_computation.3 | async-start | bytes 1310720 | tf_op jit(solution)/shard_map/all_to_all | solution.py:499
  62.7 0.0 copy-done.3
  62.7 2.2 %collective-permute-start.2 = (bf16[4,4,48,256]{3,2,1,0:T(8,128)(2,1)S(1)}, bf16[4,4,48,256]{3,2,1,0:T(8,128)(2,1)S(1)}, u32[]{:S(2)}, u32[]{:S(2)}) collective-permute-start(bf16[4,4,48,256]{3,2,1,0:T(8,128)(2,1)S(1)} %pad_maximum_fusion.refs_4_), channel_id=1, source_target_pairs={{0,4},{4,0},{1,5},{5,1},{2,6},{6,2},{3,7},{7,3},{8,12},{12,8},{9,1... | collective-permute-start | bytes 1179656 | tf_op jit(solution)/shard_map/ppermute | solution.py:484
  64.9 1.4 %collective-permute-done.2.refs_5_ = bf16[4,4,48,256]{3,2,1,0:T(8,128)(2,1)S(1)} collective-permute-done((bf16[4,4,48,256]{3,2,1,0:T(8,128)(2,1)S(1)}, bf16[4,4,48,256]{3,2,1,0:T(8,128)(2,1)S(1)}, u32[]{:S(2)}, u32[]{:S(2)}) %collective-permute-start.2) | collective-permute-done | bytes 393248 | tf_op jit(solution)/shard_map/ppermute | solution.py:484
  66.4 0.0 copy-start.4
  66.4 9.5 %all-to-all-done.3 = bf16[32,40,256]{2,1,0:T(8,128)(2,1)S(1)} async-done(((bf16[32,40,256]{2,1,0:T(8,128)(2,1)}), bf16[32,40,256]{2,1,0:T(8,128)(2,1)S(1)}, u32[]{:S(2)}, u32[]{:S(2)}) %all-to-all-start.3) | async-done | bytes 655392 | tf_op jit(solution)/shard_map/all_to_all | solution.py:499
  75.8 0.0 copy-done.4
  75.8 0.0 copy-done
  75.8 0.0 copy-done.1
  75.8 2.6 %experts.1 = bf16[8,4,40,256]{3,2,1,0:T(8,128)(2,1)} custom-call(bf16[8,4,40,256]{3,2,1,0:T(8,128)(2,1)S(1)} %bitcast.18, bf16[1,1024,256]{2,1,0:T(8,128)(2,1)S(1)} %copy-done, bf16[1,1024,256]{2,1,0:T(8,128)(2,1)S(1)} %copy-done.1, bf16[1,256,1024]{2,1,0:T(8,128)(2,1)} %refs_3_.3, bf16[4,4,48,256]{3,2,1,0:T(8,128)(2,1)} %copy-done.3, ...), custom_call_target="tpu_custom_call" | custom-call | tf_op jit(solution)/shard_map/experts/pallas_call | solution.py:513
  78.4 3.9 %all-to-all-start.4 = ((bf16[32,40,256]{2,1,0:T(8,128)(2,1)}), bf16[32,40,256]{2,1,0:T(8,128)(2,1)S(1)}, u32[]{:S(2)}, u32[]{:S(2)}) async-start(bf16[32,40,256]{2,1,0:T(8,128)(2,1)} %bitcast.21), calls=%async_computation.4 | async-start | bytes 1310720 | tf_op jit(solution)/shard_map/all_to_all | solution.py:534
  82.4 0.9 weights.1
  83.2 12.2 %all-to-all-done.4 = bf16[32,40,256]{2,1,0:T(8,128)(2,1)S(1)} async-done(((bf16[32,40,256]{2,1,0:T(8,128)(2,1)}), bf16[32,40,256]{2,1,0:T(8,128)(2,1)S(1)}, u32[]{:S(2)}, u32[]{:S(2)}) %all-to-all-start.4) | async-done | bytes 655392 | tf_op jit(solution)/shard_map/all_to_all | solution.py:534
  95.5 0.3 inward.1
  95.7 25.4 %all_to_all.30 = bf16[16,16,256]{2,1,0:T(8,128)(2,1)S(1)} all-to-all(bf16[16,16,256]{2,1,0:T(8,128)(2,1)S(1)} %inward.1), channel_id=1, replica_groups=mesh['ep_0'=16,'ep_1'=4,'ep_2'=2,'tp'=4] {'ep_0'}, dimensions={0} | all-to-all | bytes 262144 | tf_op jit(solution)/shard_map/all_to_all | solution.py:543
  121.1 0.6 add_convert_fusion
  (4 shorter events, 0.1 us)
Async XLA Ops:
  2.1 10.5 %all-to-all-start = ((bf16[4,72,256]{2,1,0:T(8,128)(2,1)}), bf16[4,72,256]{2,1,0:T(8,128)(2,1)S(1)}, u32[]{:S(2)}, u32[]{:S(2)}) async-start(bf16[4,72,256]{2,1,0:T(8,128)(2,1)} %opening.1), calls=%async_computation | async-start | bytes 294912 | tf_op jit(solution)/shard_map/all_to_all | solution.py:414
  7.2 0.7 copy-start.6
  14.8 9.3 %all-to-all-start.1 = ((bf16[4,16,1024]{2,1,0:T(8,128)(2,1)}), bf16[4,16,1024]{2,1,0:T(8,128)(2,1)S(1)}, u32[]{:S(2)}, u32[]{:S(2)}) async-start(bf16[4,16,1024]{2,1,0:T(8,128)(2,1)} %get-tuple-element.34), calls=%async_computation.1 | async-start | bytes 262144 | tf_op jit(solution)/shard_map/all_to_all | solution.py:457
  18.2 0.7 copy-start.2
  18.9 0.7 copy-start.5
  25.0 30.9 %all-to-all-start.2 = ((bf16[16,40,128]{2,1,0:T(8,128)(2,1)}), bf16[16,40,128]{2,1,0:T(8,128)(2,1)S(1)}, u32[]{:S(2)}, u32[]{:S(2)}) async-start(bf16[16,40,128]{2,1,0:T(8,128)(2,1)} %get-tuple-element.37), calls=%async_computation.2 | async-start | bytes 327680 | tf_op jit(solution)/shard_map/all_to_all | solution.py:479
  40.2 8.0 %collective-permute-start = (bf16[1,4,48,256]{3,2,1,0:T(8,128)(2,1)S(1)}, bf16[1,4,48,256]{3,2,1,0:T(8,128)(2,1)S(1)}, u32[]{:S(2)}, u32[]{:S(2)}) collective-permute-start(bf16[1,4,48,256]{3,2,1,0:T(8,128)(2,1)S(1)} %slice_bitcast_fusion), channel_id=1, source_target_pairs={{0,16},{8,24},{16,0},{24,8},{1,17},{9,25},{17,1},{25,9},{2,18},{10... | collective-permute-start | bytes 294920 | tf_op jit(solution)/shard_map/ppermute | solution.py:357
  48.2 7.6 %collective-permute-start.1 = (bf16[2,4,48,256]{3,2,1,0:T(8,128)(2,1)S(1)}, bf16[2,4,48,256]{3,2,1,0:T(8,128)(2,1)S(1)}, u32[]{:S(2)}, u32[]{:S(2)}) collective-permute-start(bf16[2,4,48,256]{3,2,1,0:T(8,128)(2,1)S(1)} %pad_maximum_fusion.1), channel_id=1, source_target_pairs={{0,8},{8,0},{16,24},{24,16},{1,9},{9,1},{17,25},{25,17},{2,10},{10... | collective-permute-start | bytes 589832 | tf_op jit(solution)/shard_map/ppermute | solution.py:357
  55.8 6.9 %copy-start.3 = (bf16[4,4,48,256]{3,2,1,0:T(8,128)(2,1)}, bf16[4,4,48,256]{3,2,1,0:T(8,128)(2,1)S(1)}, u32[]{:S(2)}) copy-start(bf16[4,4,48,256]{3,2,1,0:T(8,128)(2,1)S(1)} %pad_maximum_fusion.refs_4_) | copy-start | bytes 1179652
  57.3 18.6 %copy-start = (bf16[1,1024,256]{2,1,0:T(8,128)(2,1)S(1)}, bf16[1,1024,256]{2,1,0:T(8,128)(2,1)}, u32[]{:S(2)}) copy-start(bf16[1,1024,256]{2,1,0:T(8,128)(2,1)} %refs_1_.3) | copy-start | bytes 1572868
  57.3 18.5 %copy-start.1 = (bf16[1,1024,256]{2,1,0:T(8,128)(2,1)S(1)}, bf16[1,1024,256]{2,1,0:T(8,128)(2,1)}, u32[]{:S(2)}) copy-start(bf16[1,1024,256]{2,1,0:T(8,128)(2,1)} %refs_2_.3) | copy-start | bytes 1572868
  57.3 18.5 %all-to-all-start.3 = ((bf16[32,40,256]{2,1,0:T(8,128)(2,1)}), bf16[32,40,256]{2,1,0:T(8,128)(2,1)S(1)}, u32[]{:S(2)}, u32[]{:S(2)}) async-start(bf16[32,40,256]{2,1,0:T(8,128)(2,1)} %bitcast.22), calls=%async_computation.3 | async-start | bytes 1310720 | tf_op jit(solution)/shard_map/all_to_all | solution.py:499
  62.7 3.6 %collective-permute-start.2 = (bf16[4,4,48,256]{3,2,1,0:T(8,128)(2,1)S(1)}, bf16[4,4,48,256]{3,2,1,0:T(8,128)(2,1)S(1)}, u32[]{:S(2)}, u32[]{:S(2)}) collective-permute-start(bf16[4,4,48,256]{3,2,1,0:T(8,128)(2,1)S(1)} %pad_maximum_fusion.refs_4_), channel_id=1, source_target_pairs={{0,4},{4,0},{1,5},{5,1},{2,6},{6,2},{3,7},{7,3},{8,12},{12,8},{9,1... | collective-permute-start | bytes 1179656 | tf_op jit(solution)/shard_map/ppermute | solution.py:484
  66.4 9.5 %copy-start.4 = (bf16[4,4,48,256]{3,2,1,0:T(8,128)(2,1)}, bf16[4,4,48,256]{3,2,1,0:T(8,128)(2,1)S(1)}, u32[]{:S(2)}) copy-start(bf16[4,4,48,256]{3,2,1,0:T(8,128)(2,1)S(1)} %collective-permute-done.2.refs_5_) | copy-start | bytes 1179652
  78.4 17.0 %all-to-all-start.4 = ((bf16[32,40,256]{2,1,0:T(8,128)(2,1)}), bf16[32,40,256]{2,1,0:T(8,128)(2,1)S(1)}, u32[]{:S(2)}, u32[]{:S(2)}) async-start(bf16[32,40,256]{2,1,0:T(8,128)(2,1)} %bitcast.21), calls=%async_computation.4 | async-start | bytes 1310720 | tf_op jit(solution)/shard_map/all_to_all | solution.py:534
where the time goes:
time: 123 us; the launch traced here: 122 us
  starting transfers between devices  42.9 us (35%)
  waiting for transfers between devices  37.1 us (30%)
  blocking collectives  25.4 us (21%)
  Pallas kernels  12.1 us (10%)
  local copies, waits for them, and re-layouts  2.21 us (2%)
  between operations  1.46 us (1%)
    all_to_all x1, blocking collectives, body(): home = lax.all_to_all(back, 'ep_0', 0, 0, tiled=True)  25.4 us
    all_to_all x1, starting transfers between devices, body(): seen = lax.all_to_all(message, 'ep_0', 0, 0, tiled=True)  15.2 us
    all_to_all x1, waiting for transfers between devices, body(): lax.all_to_all(sent.reshape(plane * tp, slots + dealt, width), BLOCK, 0,...  12.2 us
    all_to_all x1, waiting for transfers between devices, body(): lax.all_to_all(outward.reshape(plane * tp, slots + dealt, width), BLOCK,...  9.45 us
    ppermute x2, starting transfers between devices, doubled(): other = lax.ppermute(held, 'ep_1', [(i, i ^ step) for i in range(columns)])  8.34 us
    ppermute x2, waiting for transfers between devices, doubled(): other = lax.ppermute(held, 'ep_1', [(i, i ^ step) for i in range(columns)])  7.22 us
    all_to_all x1, starting transfers between devices, body(): lax.all_to_all(outward.reshape(plane * tp, slots + dealt, width), BLOCK,...  5.44 us
    all_to_all x1, starting transfers between devices, body(): pieces = lax.all_to_all(mine, 'tp', 0, 0, tiled=True)  4.46 us
  transfers between devices with their start and end apart: 8, of which 7 were waited for; matrix products, arithmetic and copies ran while one was open for 0% of the time, Pallas kernels for 3%

commit v1 on v0

--- a/solution.py
+++ b/solution.py
@@ -107,6 +107,18 @@
         move.start()
     for move in moves:
         move.wait()
+
+
+def brought(arrays):
+    return pl.pallas_call(
+        stage_kernel,
+        out_shape=tuple(map(kept, arrays)),
+        in_specs=[pl.BlockSpec(memory_space=pl.ANY)] * len(arrays),
+        out_specs=(WHOLE,) * len(arrays),
+        scratch_shapes=[pltpu.SemaphoreType.DMA((len(arrays),))],
+        name="stage",
+        compiler_params=LIMIT,
+    )(*map(far, arrays))
 
 
 def attend_kernel(
@@ -291,48 +303,52 @@
 
 
 def expert_kernel(
-    seen_ref, gate_ref, up_ref, down_hbm, own_hbm, other_hbm, out_hbm, down_ref, dense_ref, out_ref, sems, *, slots
+    seen_ref, gate_ref, up_ref, down_ref, own_ref, other_ref, out_hbm, out_ref, sems, *, slots
 ):
-    fetches = [
-        pltpu.make_async_copy(own_hbm, dense_ref.at[0], sems.at[0]),
-        pltpu.make_async_copy(other_hbm, dense_ref.at[1], sems.at[1]),
-        pltpu.make_async_copy(down_hbm, down_ref, sems.at[2]),
-    ]
-    for fetch in fetches:
-        fetch.start()
     plane, tp, items, width = seen_ref.shape
-    gate_pre = up_pre = 0.0
-    for k in range(tp):
-        rows = seen_ref[:, k, :slots, :].reshape(plane * slots, width)
-        gate_pre = gate_pre + mm(rows, gate_ref[0, k * width : (k + 1) * width, :])
-        up_pre = up_pre + mm(rows, up_ref[0, k * width : (k + 1) * width, :])
+    rows = jnp.concatenate(
+        [seen_ref[:, k, :slots, :].reshape(plane * slots, width) for k in range(tp)], axis=1
+    )
+    gate_pre = mm(rows, gate_ref[0])
+    up_pre = mm(rows, up_ref[0])
     act = clamped_unit(gate_pre, up_pre).astype(jnp.bfloat16)
-    _, columns, _, rows_each, _ = dense_ref.shape
+    columns, _, rows_each, _ = own_ref.shape
     units = rows_each // 3
-    every = 2 * columns * units
     dealt = items - slots
-    fetches[0].wait()
-    fetches[1].wait()
-    gate_pre = up_pre = 0.0
-    for k in range(tp):
-        rows = seen_ref[:, k, slots:, :].astype(jnp.float32).reshape(plane * dealt, width)
-        rows = rows.astype(jnp.bfloat16)
-        gate = dense_ref[:, :, k, :units, :].reshape(every, width)
-        up = dense_ref[:, :, k, units : 2 * units, :].reshape(every, width)
-        gate_pre = gate_pre + lax.dot_general(
-            rows, gate, ACROSS, preferred_element_type=jnp.float32
-        )
-        up_pre = up_pre + lax.dot_general(rows, up, ACROSS, preferred_element_type=jnp.float32)
+
+    def units_at(k, lo):
+        return jnp.concatenate(
+            [
+                ref[:, k, lo : lo + units, :].reshape(columns * units, width)
+                for ref in (own_ref, other_ref)
+            ],
+            axis=0,
+        )
+
+    rows = jnp.concatenate(
+        [
+            seen_ref[:, k, slots:, :].astype(jnp.float32).reshape(plane * dealt, width)
+            for k in range(tp)
+        ],
+        axis=1,
+    ).astype(jnp.bfloat16)
+
+    def units_of(lo):
+        return jnp.concatenate(
+            [units_at(k, lo) for k in range(tp)],
+            axis=1,
+        )
+
+    gate_pre = lax.dot_general(rows, units_of(0), ACROSS, preferred_element_type=jnp.float32)
+    up_pre = lax.dot_general(rows, units_of(units), ACROSS, preferred_element_type=jnp.float32)
     dense_act = (gate_pre / (1.0 + jnp.exp(-gate_pre)) * up_pre).astype(jnp.bfloat16)
-    fetches[2].wait()
     moves = []
     for k in range(tp):
         part = mm(act, down_ref[0, :, k * width : (k + 1) * width]).astype(jnp.bfloat16)
         out_ref[k, :, :slots, :] = part.reshape(plane, slots, width)
-        down = dense_ref[:, :, k, 2 * units :, :].reshape(every, width)
-        part = mm(dense_act, down).reshape(plane, dealt, width)
+        part = mm(dense_act, units_at(k, 2 * units)).reshape(plane, dealt, width)
         out_ref[k, :, slots:, :] = part.astype(jnp.bfloat16)
-        moves.append(pltpu.make_async_copy(out_ref.at[k], out_hbm.at[:, k], sems.at[3 + k]))
+        moves.append(pltpu.make_async_copy(out_ref.at[k], out_hbm.at[:, k], sems.at[k]))
         moves[-1].start()
     for move in moves:
         move.wait()
@@ -425,15 +441,7 @@
         cache_value,
         norm_gain_mix[None, :],
     )
-    *staged, gain_here = pl.pallas_call(
-        stage_kernel,
-        out_shape=tuple(map(kept, needed)),
-        in_specs=[pl.BlockSpec(memory_space=pl.ANY)] * len(needed),
-        out_specs=(WHOLE,) * len(needed),
-        scratch_shapes=[pltpu.SemaphoreType.DMA((len(needed),))],
-        name="stage",
-        compiler_params=LIMIT,
-    )(*map(far, needed))
+    *staged, gain_here = brought(needed)
     routes = pl.pallas_call(
         routes_kernel, out_shape=shaped((seq, LANES), jnp.float32), name="routes", compiler_params=LIMIT
     )(route_ids, route_ids.T, route_logits)
@@ -510,26 +518,21 @@
         name="weights",
         compiler_params=LIMIT,
     )(first, seen)
+    tools = brought((expert_gate, expert_up, expert_down, own_dense, other_dense))
     sent = pl.pallas_call(
         lambda *refs: expert_kernel(*refs, slots=slots),
         out_shape=sent_to_hbm((plane, tp, slots + dealt, width), jnp.bfloat16),
-        in_specs=[WHOLE] * 3 + [pl.BlockSpec(memory_space=pl.ANY)] * 3,
+        in_specs=[WHOLE] * 6,
         out_specs=pl.BlockSpec(memory_space=pl.ANY),
         scratch_shapes=[
-            pltpu.VMEM(expert_down.shape, expert_down.dtype),
-            pltpu.VMEM((2, *own_dense.shape), own_dense.dtype),
             pltpu.VMEM((tp, plane, slots + dealt, width), jnp.bfloat16),
-            pltpu.SemaphoreType.DMA((3 + tp,)),
+            pltpu.SemaphoreType.DMA((tp,)),
         ],
         name="experts",
         compiler_params=LIMIT,
     )(
         near(arrived),
-        near(expert_gate),
-        near(expert_up),
-        far(expert_down),
-        far(own_dense),
-        far(other_dense),
+        *map(near, tools),
     )
     returned = lax.all_to_all(
         sent.reshape(plane * tp, slots + dealt, width), BLOCK, 0, 0, tiled=True

time: 123 us -> 122 us (level)
  waiting for transfers between devices: 37.1 us -> 34.7 us
    all_to_all x1, waiting for transfers between devices: 9.45 us -> 7.05 us  [body(): lax.all_to_all(outward.reshape(plane * tp, slots + dealt, width), BLOCK,...]
    pallas_call x1 -> x2, Pallas kernels: 2.02 us -> 3.67 us  [brought(): pl.pallas_call(stage_kernel, out_shape=tuple(map(kept, arrays)), in_specs...]
    unnamed x16 -> x12, local copies, waits for them, and re-layouts: 2.12 us -> 2.87 us
  transfers between devices with their start and end apart: 8 -> 8, of which waited for: 7 -> 7; matrix products, arithmetic and copies ran while one was open for 0% -> 0% of each run, Pallas kernels for 3% -> 4%
where the time goes in v1:
time: 122 us; the launch traced here: 121 us
  starting transfers between devices  42.7 us (35%)
  waiting for transfers between devices  34.7 us (28%)
  blocking collectives  25.4 us (21%)
  Pallas kernels  12.8 us (10%)
  local copies, waits for them, and re-layouts  2.96 us (2%)
  between operations  1.44 us (1%)
    all_to_all x1, blocking collectives, body(): home = lax.all_to_all(back, 'ep_0', 0, 0, tiled=True)  25.4 us
    all_to_all x1, starting transfers between devices, body(): seen = lax.all_to_all(message, 'ep_0', 0, 0, tiled=True)  15.2 us
    all_to_all x1, waiting for transfers between devices, body(): lax.all_to_all(sent.reshape(plane * tp, slots + dealt, width), BLOCK, 0,...  12.2 us
    ppermute x2, starting transfers between devices, doubled(): other = lax.ppermute(held, 'ep_1', [(i, i ^ step) for i in range(columns)])  8.33 us
    ppermute x2, waiting for transfers between devices, doubled(): other = lax.ppermute(held, 'ep_1', [(i, i ^ step) for i in range(columns)])  7.23 us
    all_to_all x1, waiting for transfers between devices, body(): lax.all_to_all(outward.reshape(plane * tp, slots + dealt, width), BLOCK,...  7.05 us
    all_to_all x1, starting transfers between devices, body(): lax.all_to_all(outward.reshape(plane * tp, slots + dealt, width), BLOCK,...  5.31 us
    all_to_all x1, starting transfers between devices, body(): pieces = lax.all_to_all(mine, 'tp', 0, 0, tiled=True)  4.46 us
  transfers between devices with their start and end apart: 8, of which 7 were waited for; matrix products, arithmetic and copies ran while one was open for 0% of the time, Pallas kernels for 4%

profile of v1, /device:TPU:32, one launch (start us, length us, event | category | flops | bytes accessed | tf_op | source)
XLA Modules:
  0.0 120.7 jit_solution(10605116021044016399)
XLA Ops:
  0.6 1.4 %opening.1 = bf16[4,72,256]{2,1,0:T(8,128)(2,1)} custom-call(bf16[16,256]{1,0:T(8,128)(2,1)} %hidden_ref.1, bf16[16,256]{1,0:T(8,128)(2,1)} %bitcast.23, bf16[16,256]{1,0:T(8,128)(2,1)} %bitcast.24, bf16[16,256]{1,0:T(8,128)(2,1)} %down_ref.1, f32[1,256]{1,0:T(1,128)} %bitcast.26, f32[1,256]{1,0:T(1,128)} %bitcast.28), custom_call_target="tpu_custom_call" | custom-call | tf_op jit(solution)/shard_map/opening/pallas_call | solution.py:415
  2.1 4.5 %all-to-all-start = ((bf16[4,72,256]{2,1,0:T(8,128)(2,1)}), bf16[4,72,256]{2,1,0:T(8,128)(2,1)S(1)}, u32[]{:S(2)}, u32[]{:S(2)}) async-start(bf16[4,72,256]{2,1,0:T(8,128)(2,1)} %opening.1), calls=%async_computation | async-start | bytes 294912 | tf_op jit(solution)/shard_map/all_to_all | solution.py:430
  6.5 0.0 copy-start.4
  6.5 0.7 copy-done.4
  7.2 0.1 copy.26.lengths_ref
  7.9 2.0 %stage.2 = (f32[1,1024]{1,0:T(1,128)S(1)}, bf16[1024,128]{1,0:T(8,128)(2,1)S(1)}, bf16[1024,128]{1,0:T(8,128)(2,1)S(1)}, bf16[1024,128]{1,0:T(8,128)(2,1)S(1)}, ...) custom-call(f32[1,1024]{1,0:T(1,128)} %bitcast.25, ...), custom_call_target="tpu_custom_call" | custom-call | tf_op jit(solution)/shard_map/stage/pallas_call | solution.py:113
  10.0 2.6 %all-to-all-done.pieces_ref.refs_2_ = bf16[4,72,256]{2,1,0:T(8,128)(2,1)S(1)} async-done(((bf16[4,72,256]{2,1,0:T(8,128)(2,1)}), bf16[4,72,256]{2,1,0:T(8,128)(2,1)S(1)}, u32[]{:S(2)}, u32[]{:S(2)}) %all-to-all-start) | async-done | bytes 147488 | tf_op jit(solution)/shard_map/all_to_all | solution.py:430
  12.6 2.3 %attend.1 = (bf16[4,16,1024]{2,1,0:T(8,128)(2,1)}, bf16[16,128]{1,0:T(8,128)(2,1)}, bf16[16,128]{1,0:T(8,128)(2,1)}) custom-call(f32[1]{0:T(128)S(6)} %copy.29.lambda_ref, bf16[4,72,256]{2,1,0:T(8,128)(2,1)S(1)} %all-to-all-done.pieces_ref.refs_2_, f32[1,1024]{1,0:T(1,128)S(1)} %get-tuple-element.29.gain_ref, ...), custom_call_target="tpu_custom_call" | custom-call | tf_op jit(solution)/shard_map/attend/pallas_call | solution.py:449
  14.8 3.3 %all-to-all-start.1 = ((bf16[4,16,1024]{2,1,0:T(8,128)(2,1)}), bf16[4,16,1024]{2,1,0:T(8,128)(2,1)S(1)}, u32[]{:S(2)}, u32[]{:S(2)}) async-start(bf16[4,16,1024]{2,1,0:T(8,128)(2,1)} %get-tuple-element.39), calls=%async_computation.1 | async-start | bytes 262144 | tf_op jit(solution)/shard_map/all_to_all | solution.py:465
  18.2 0.0 copy-start
  18.2 0.7 copy-done
  18.9 0.0 copy-start.3
  18.9 0.1 copy.27.ids_ref
  18.9 0.6 copy-done.3
  19.5 0.1 copy.28.logits_ref
  19.6 0.4 routes.1.refs_4_
  20.0 4.1 %all-to-all-done.1.refs_1_ = bf16[4,16,1024]{2,1,0:T(8,128)(2,1)S(1)} async-done(((bf16[4,16,1024]{2,1,0:T(8,128)(2,1)}), bf16[4,16,1024]{2,1,0:T(8,128)(2,1)S(1)}, u32[]{:S(2)}, u32[]{:S(2)}) %all-to-all-start.1) | async-done | bytes 131104 | tf_op jit(solution)/shard_map/all_to_all | solution.py:465
  24.1 0.9 mix.1
  25.0 15.2 %all-to-all-start.2 = ((bf16[16,40,128]{2,1,0:T(8,128)(2,1)}), bf16[16,40,128]{2,1,0:T(8,128)(2,1)S(1)}, u32[]{:S(2)}, u32[]{:S(2)}) async-start(bf16[16,40,128]{2,1,0:T(8,128)(2,1)} %get-tuple-element.42), calls=%async_computation.2 | async-start | bytes 327680 | tf_op jit(solution)/shard_map/all_to_all | solution.py:487
  40.2 4.9 %collective-permute-start = (bf16[1,4,48,256]{3,2,1,0:T(8,128)(2,1)S(1)}, bf16[1,4,48,256]{3,2,1,0:T(8,128)(2,1)S(1)}, u32[]{:S(2)}, u32[]{:S(2)}) collective-permute-start(bf16[1,4,48,256]{3,2,1,0:T(8,128)(2,1)S(1)} %slice_bitcast_fusion), channel_id=1, source_target_pairs={{0,16},{8,24},{16,0},{24,8},{1,17},{9,25},{17,1},{25,9},{2,18},{10... | collective-permute-start | bytes 294920 | tf_op jit(solution)/shard_map/ppermute | solution.py:373
  45.1 3.1 %collective-permute-done = bf16[1,4,48,256]{3,2,1,0:T(8,128)(2,1)S(1)} collective-permute-done((bf16[1,4,48,256]{3,2,1,0:T(8,128)(2,1)S(1)}, bf16[1,4,48,256]{3,2,1,0:T(8,128)(2,1)S(1)}, u32[]{:S(2)}, u32[]{:S(2)}) %collective-permute-start) | collective-permute-done | bytes 98336 | tf_op jit(solution)/shard_map/ppermute | solution.py:373
  48.2 3.4 %collective-permute-start.1 = (bf16[2,4,48,256]{3,2,1,0:T(8,128)(2,1)S(1)}, bf16[2,4,48,256]{3,2,1,0:T(8,128)(2,1)S(1)}, u32[]{:S(2)}, u32[]{:S(2)}) collective-permute-start(bf16[2,4,48,256]{3,2,1,0:T(8,128)(2,1)S(1)} %pad_maximum_fusion.1), channel_id=1, source_target_pairs={{0,8},{8,0},{16,24},{24,16},{1,9},{9,1},{17,25},{25,17},{2,10},{10... | collective-permute-start | bytes 589832 | tf_op jit(solution)/shard_map/ppermute | solution.py:373
  51.6 4.2 %collective-permute-done.1 = bf16[2,4,48,256]{3,2,1,0:T(8,128)(2,1)S(1)} collective-permute-done((bf16[2,4,48,256]{3,2,1,0:T(8,128)(2,1)S(1)}, bf16[2,4,48,256]{3,2,1,0:T(8,128)(2,1)S(1)}, u32[]{:S(2)}, u32[]{:S(2)}) %collective-permute-start.1) | collective-permute-done | bytes 196640 | tf_op jit(solution)/shard_map/ppermute | solution.py:373
  55.8 0.0 copy-start.1
  55.9 0.0 all-to-all-done.2.refs_1_
  55.9 1.4 %outward.1 = bf16[8,4,40,256]{3,2,1,0:T(8,128)(2,1)} custom-call(s32[1]{0:T(128)} %bitcast.11.refs_0_, bf16[16,40,128]{2,1,0:T(8,128)(2,1)S(1)} %all-to-all-done.2.refs_1_), custom_call_target="tpu_custom_call" | custom-call | tf_op jit(solution)/shard_map/outward/pallas_call | solution.py:494
  57.3 5.3 %all-to-all-start.3 = ((bf16[32,40,256]{2,1,0:T(8,128)(2,1)}), bf16[32,40,256]{2,1,0:T(8,128)(2,1)S(1)}, u32[]{:S(2)}, u32[]{:S(2)}) async-start(bf16[32,40,256]{2,1,0:T(8,128)(2,1)} %bitcast.22), calls=%async_computation.3 | async-start | bytes 1310720 | tf_op jit(solution)/shard_map/all_to_all | solution.py:507
  62.6 0.0 copy-done.1
  62.6 2.2 %collective-permute-start.2 = (bf16[4,4,48,256]{3,2,1,0:T(8,128)(2,1)S(1)}, bf16[4,4,48,256]{3,2,1,0:T(8,128)(2,1)S(1)}, u32[]{:S(2)}, u32[]{:S(2)}) collective-permute-start(bf16[4,4,48,256]{3,2,1,0:T(8,128)(2,1)S(1)} %pad_maximum_fusion.refs_3_), channel_id=1, source_target_pairs={{0,4},{4,0},{1,5},{5,1},{2,6},{6,2},{3,7},{7,3},{8,12},{12,8},{9,1... | collective-permute-start | bytes 1179656 | tf_op jit(solution)/shard_map/ppermute | solution.py:492
  64.8 1.4 %collective-permute-done.2.refs_4_ = bf16[4,4,48,256]{3,2,1,0:T(8,128)(2,1)S(1)} collective-permute-done((bf16[4,4,48,256]{3,2,1,0:T(8,128)(2,1)S(1)}, bf16[4,4,48,256]{3,2,1,0:T(8,128)(2,1)S(1)}, u32[]{:S(2)}, u32[]{:S(2)}) %collective-permute-start.2) | collective-permute-done | bytes 393248 | tf_op jit(solution)/shard_map/ppermute | solution.py:492
  66.2 0.0 copy-start.2
  66.2 0.8 copy-done.2
  67.0 1.6 %stage.3 = (bf16[1,1024,256]{2,1,0:T(8,128)(2,1)S(1)}, bf16[1,1024,256]{2,1,0:T(8,128)(2,1)S(1)}, bf16[1,256,1024]{2,1,0:T(8,128)(2,1)S(1)}, bf16[4,4,48,256]{3,...) custom-call(bf16[1,1024,256]{2,1,0:T(8,128)(2,1)} %refs_0_.1, bf16[1,1024,256]{2,1,0:T(8,128)(2,1)} %refs_1_.3, ...), custom_call_target="tpu_custom_call" | custom-call | tf_op jit(solution)/shard_map/stage/pallas_call | solution.py:113
  68.6 7.1 %all-to-all-done.3 = bf16[32,40,256]{2,1,0:T(8,128)(2,1)S(1)} async-done(((bf16[32,40,256]{2,1,0:T(8,128)(2,1)}), bf16[32,40,256]{2,1,0:T(8,128)(2,1)S(1)}, u32[]{:S(2)}, u32[]{:S(2)}) %all-to-all-start.3) | async-done | bytes 655392 | tf_op jit(solution)/shard_map/all_to_all | solution.py:507
  75.7 1.7 %experts.1 = bf16[8,4,40,256]{3,2,1,0:T(8,128)(2,1)} custom-call(bf16[8,4,40,256]{3,2,1,0:T(8,128)(2,1)S(1)} %bitcast.18, bf16[1,1024,256]{2,1,0:T(8,128)(2,1)S(1)} %get-tuple-element.45.refs_1_, bf16[1,1024,256]{2,1,0:T(8,128)(2,1)S(1)} %get-tuple-element.46.refs_2_, bf16[1,256,1024]{2,1,0:T(8,128)(2,1)S(1)} %get-tuple-element.47.refs_3_, ...), custom_call_target="tpu_custom_call" | custom-call | tf_op jit(solution)/shard_map/experts/pallas_call | solution.py:522
  77.4 3.9 %all-to-all-start.4 = ((bf16[32,40,256]{2,1,0:T(8,128)(2,1)}), bf16[32,40,256]{2,1,0:T(8,128)(2,1)S(1)}, u32[]{:S(2)}, u32[]{:S(2)}) async-start(bf16[32,40,256]{2,1,0:T(8,128)(2,1)} %bitcast.21), calls=%async_computation.4 | async-start | bytes 1310720 | tf_op jit(solution)/shard_map/all_to_all | solution.py:537
  81.3 0.9 weights.1
  82.1 12.2 %all-to-all-done.4 = bf16[32,40,256]{2,1,0:T(8,128)(2,1)S(1)} async-done(((bf16[32,40,256]{2,1,0:T(8,128)(2,1)}), bf16[32,40,256]{2,1,0:T(8,128)(2,1)S(1)}, u32[]{:S(2)}, u32[]{:S(2)}) %all-to-all-start.4) | async-done | bytes 655392 | tf_op jit(solution)/shard_map/all_to_all | solution.py:537
  94.4 0.3 inward.1
  94.6 25.4 %all_to_all.30 = bf16[16,16,256]{2,1,0:T(8,128)(2,1)S(1)} all-to-all(bf16[16,16,256]{2,1,0:T(8,128)(2,1)S(1)} %inward.1), channel_id=1, replica_groups=mesh['ep_0'=16,'ep_1'=4,'ep_2'=2,'tp'=4] {'ep_0'}, dimensions={0} | all-to-all | bytes 262144 | tf_op jit(solution)/shard_map/all_to_all | solution.py:546
  120.1 0.6 add_convert_fusion
  (4 shorter events, 0.1 us)
Async XLA Ops:
  2.1 10.5 %all-to-all-start = ((bf16[4,72,256]{2,1,0:T(8,128)(2,1)}), bf16[4,72,256]{2,1,0:T(8,128)(2,1)S(1)}, u32[]{:S(2)}, u32[]{:S(2)}) async-start(bf16[4,72,256]{2,1,0:T(8,128)(2,1)} %opening.1), calls=%async_computation | async-start | bytes 294912 | tf_op jit(solution)/shard_map/all_to_all | solution.py:430
  6.5 0.7 copy-start.4
  14.8 9.3 %all-to-all-start.1 = ((bf16[4,16,1024]{2,1,0:T(8,128)(2,1)}), bf16[4,16,1024]{2,1,0:T(8,128)(2,1)S(1)}, u32[]{:S(2)}, u32[]{:S(2)}) async-start(bf16[4,16,1024]{2,1,0:T(8,128)(2,1)} %get-tuple-element.39), calls=%async_computation.1 | async-start | bytes 262144 | tf_op jit(solution)/shard_map/all_to_all | solution.py:465
  18.2 0.7 copy-start
  18.9 0.7 copy-start.3
  25.0 30.9 %all-to-all-start.2 = ((bf16[16,40,128]{2,1,0:T(8,128)(2,1)}), bf16[16,40,128]{2,1,0:T(8,128)(2,1)S(1)}, u32[]{:S(2)}, u32[]{:S(2)}) async-start(bf16[16,40,128]{2,1,0:T(8,128)(2,1)} %get-tuple-element.42), calls=%async_computation.2 | async-start | bytes 327680 | tf_op jit(solution)/shard_map/all_to_all | solution.py:487
  40.2 8.0 %collective-permute-start = (bf16[1,4,48,256]{3,2,1,0:T(8,128)(2,1)S(1)}, bf16[1,4,48,256]{3,2,1,0:T(8,128)(2,1)S(1)}, u32[]{:S(2)}, u32[]{:S(2)}) collective-permute-start(bf16[1,4,48,256]{3,2,1,0:T(8,128)(2,1)S(1)} %slice_bitcast_fusion), channel_id=1, source_target_pairs={{0,16},{8,24},{16,0},{24,8},{1,17},{9,25},{17,1},{25,9},{2,18},{10... | collective-permute-start | bytes 294920 | tf_op jit(solution)/shard_map/ppermute | solution.py:373
  48.2 7.6 %collective-permute-start.1 = (bf16[2,4,48,256]{3,2,1,0:T(8,128)(2,1)S(1)}, bf16[2,4,48,256]{3,2,1,0:T(8,128)(2,1)S(1)}, u32[]{:S(2)}, u32[]{:S(2)}) collective-permute-start(bf16[2,4,48,256]{3,2,1,0:T(8,128)(2,1)S(1)} %pad_maximum_fusion.1), channel_id=1, source_target_pairs={{0,8},{8,0},{16,24},{24,16},{1,9},{9,1},{17,25},{25,17},{2,10},{10... | collective-permute-start | bytes 589832 | tf_op jit(solution)/shard_map/ppermute | solution.py:373
  55.8 6.8 %copy-start.1 = (bf16[4,4,48,256]{3,2,1,0:T(8,128)(2,1)}, bf16[4,4,48,256]{3,2,1,0:T(8,128)(2,1)S(1)}, u32[]{:S(2)}) copy-start(bf16[4,4,48,256]{3,2,1,0:T(8,128)(2,1)S(1)} %pad_maximum_fusion.refs_3_) | copy-start | bytes 1179652
  57.3 18.4 %all-to-all-start.3 = ((bf16[32,40,256]{2,1,0:T(8,128)(2,1)}), bf16[32,40,256]{2,1,0:T(8,128)(2,1)S(1)}, u32[]{:S(2)}, u32[]{:S(2)}) async-start(bf16[32,40,256]{2,1,0:T(8,128)(2,1)} %bitcast.22), calls=%async_computation.3 | async-start | bytes 1310720 | tf_op jit(solution)/shard_map/all_to_all | solution.py:507
  62.6 3.6 %collective-permute-start.2 = (bf16[4,4,48,256]{3,2,1,0:T(8,128)(2,1)S(1)}, bf16[4,4,48,256]{3,2,1,0:T(8,128)(2,1)S(1)}, u32[]{:S(2)}, u32[]{:S(2)}) collective-permute-start(bf16[4,4,48,256]{3,2,1,0:T(8,128)(2,1)S(1)} %pad_maximum_fusion.refs_3_), channel_id=1, source_target_pairs={{0,4},{4,0},{1,5},{5,1},{2,6},{6,2},{3,7},{7,3},{8,12},{12,8},{9,1... | collective-permute-start | bytes 1179656 | tf_op jit(solution)/shard_map/ppermute | solution.py:492
  66.2 0.8 copy-start.2
  77.4 17.0 %all-to-all-start.4 = ((bf16[32,40,256]{2,1,0:T(8,128)(2,1)}), bf16[32,40,256]{2,1,0:T(8,128)(2,1)S(1)}, u32[]{:S(2)}, u32[]{:S(2)}) async-start(bf16[32,40,256]{2,1,0:T(8,128)(2,1)} %bitcast.21), calls=%async_computation.4 | async-start | bytes 1310720 | tf_op jit(solution)/shard_map/all_to_all | solution.py:537

commit v2 on v1

--- a/solution.py
+++ b/solution.py
@@ -11,6 +11,7 @@
 
 
 EP = ("ep_0", "ep_1", "ep_2")
+PLANE = ("ep_1", "ep_2")
 BLOCK = ("ep_1", "ep_2", "tp")
 CAP = 2
 
@@ -369,8 +370,12 @@
 
 
 def doubled(held, step):
-    columns = lax.axis_size("ep_1")
-    other = lax.ppermute(held, "ep_1", [(i, i ^ step) for i in range(columns)])
+    columns, cores = lax.axis_size("ep_1"), lax.axis_size("ep_2")
+    flips = [step, step | 2 * step if 2 * step < columns else step]
+    pairs = [
+        (i * cores + c, (i ^ flips[c % 2]) * cores + c) for i in range(columns) for c in range(cores)
+    ]
+    other = lax.ppermute(held, PLANE, pairs)
     return jnp.concatenate([held, other], axis=0)
 
 

time: 122 us -> 122 us (level)
  no operation moved by 1% of the time
where the time goes in v2:
time: 122 us; the launch traced here: 121 us
  starting transfers between devices  42.7 us (35%)
  waiting for transfers between devices  34.7 us (28%)
  blocking collectives  25.4 us (21%)
  Pallas kernels  12.8 us (10%)
  local copies, waits for them, and re-layouts  2.96 us (2%)
  between operations  1.44 us (1%)
    all_to_all x1, blocking collectives, body(): home = lax.all_to_all(back, 'ep_0', 0, 0, tiled=True)  25.4 us
    all_to_all x1, starting transfers between devices, body(): seen = lax.all_to_all(message, 'ep_0', 0, 0, tiled=True)  15.2 us
    all_to_all x1, waiting for transfers between devices, body(): lax.all_to_all(sent.reshape(plane * tp, slots + dealt, width), BLOCK, 0,...  12.2 us
    ppermute x2, starting transfers between devices, doubled(): other = lax.ppermute(held, PLANE, pairs)  8.33 us
    ppermute x2, waiting for transfers between devices, doubled(): other = lax.ppermute(held, PLANE, pairs)  7.23 us
    all_to_all x1, waiting for transfers between devices, body(): lax.all_to_all(outward.reshape(plane * tp, slots + dealt, width), BLOCK,...  7.05 us
    all_to_all x1, starting transfers between devices, body(): lax.all_to_all(outward.reshape(plane * tp, slots + dealt, width), BLOCK,...  5.31 us
    all_to_all x1, starting transfers between devices, body(): pieces = lax.all_to_all(mine, 'tp', 0, 0, tiled=True)  4.46 us
  transfers between devices with their start and end apart: 8, of which 7 were waited for; matrix products, arithmetic and copies ran while one was open for 0% of the time, Pallas kernels for 4%

profile of v2, /device:TPU:32, one launch (start us, length us, event | category | flops | bytes accessed | tf_op | source)
XLA Modules:
  0.0 120.7 jit_solution(3881066863239134003)
XLA Ops:
  0.6 1.4 %opening.1 = bf16[4,72,256]{2,1,0:T(8,128)(2,1)} custom-call(bf16[16,256]{1,0:T(8,128)(2,1)} %hidden_ref.1, bf16[16,256]{1,0:T(8,128)(2,1)} %bitcast.23, bf16[16,256]{1,0:T(8,128)(2,1)} %bitcast.24, bf16[16,256]{1,0:T(8,128)(2,1)} %down_ref.1, f32[1,256]{1,0:T(1,128)} %bitcast.26, f32[1,256]{1,0:T(1,128)} %bitcast.28), custom_call_target="tpu_custom_call" | custom-call | tf_op jit(solution)/shard_map/opening/pallas_call | solution.py:420
  2.1 4.5 %all-to-all-start = ((bf16[4,72,256]{2,1,0:T(8,128)(2,1)}), bf16[4,72,256]{2,1,0:T(8,128)(2,1)S(1)}, u32[]{:S(2)}, u32[]{:S(2)}) async-start(bf16[4,72,256]{2,1,0:T(8,128)(2,1)} %opening.1), calls=%async_computation | async-start | bytes 294912 | tf_op jit(solution)/shard_map/all_to_all | solution.py:435
  6.5 0.0 copy-start.4
  6.5 0.7 copy-done.4
  7.2 0.1 copy.26.lengths_ref
  7.9 2.0 %stage.2 = (f32[1,1024]{1,0:T(1,128)S(1)}, bf16[1024,128]{1,0:T(8,128)(2,1)S(1)}, bf16[1024,128]{1,0:T(8,128)(2,1)S(1)}, bf16[1024,128]{1,0:T(8,128)(2,1)S(1)}, ...) custom-call(f32[1,1024]{1,0:T(1,128)} %bitcast.25, ...), custom_call_target="tpu_custom_call" | custom-call | tf_op jit(solution)/shard_map/stage/pallas_call | solution.py:114
  10.0 2.6 %all-to-all-done.pieces_ref.refs_2_ = bf16[4,72,256]{2,1,0:T(8,128)(2,1)S(1)} async-done(((bf16[4,72,256]{2,1,0:T(8,128)(2,1)}), bf16[4,72,256]{2,1,0:T(8,128)(2,1)S(1)}, u32[]{:S(2)}, u32[]{:S(2)}) %all-to-all-start) | async-done | bytes 147488 | tf_op jit(solution)/shard_map/all_to_all | solution.py:435
  12.6 2.3 %attend.1 = (bf16[4,16,1024]{2,1,0:T(8,128)(2,1)}, bf16[16,128]{1,0:T(8,128)(2,1)}, bf16[16,128]{1,0:T(8,128)(2,1)}) custom-call(f32[1]{0:T(128)S(6)} %copy.29.lambda_ref, bf16[4,72,256]{2,1,0:T(8,128)(2,1)S(1)} %all-to-all-done.pieces_ref.refs_2_, f32[1,1024]{1,0:T(1,128)S(1)} %get-tuple-element.29.gain_ref, ...), custom_call_target="tpu_custom_call" | custom-call | tf_op jit(solution)/shard_map/attend/pallas_call | solution.py:454
  14.8 3.3 %all-to-all-start.1 = ((bf16[4,16,1024]{2,1,0:T(8,128)(2,1)}), bf16[4,16,1024]{2,1,0:T(8,128)(2,1)S(1)}, u32[]{:S(2)}, u32[]{:S(2)}) async-start(bf16[4,16,1024]{2,1,0:T(8,128)(2,1)} %get-tuple-element.39), calls=%async_computation.1 | async-start | bytes 262144 | tf_op jit(solution)/shard_map/all_to_all | solution.py:470
  18.2 0.0 copy-start
  18.2 0.7 copy-done
  18.9 0.0 copy-start.3
  18.9 0.1 copy.27.ids_ref
  18.9 0.6 copy-done.3
  19.5 0.1 copy.28.logits_ref
  19.6 0.4 routes.1.refs_4_
  20.0 4.1 %all-to-all-done.1.refs_1_ = bf16[4,16,1024]{2,1,0:T(8,128)(2,1)S(1)} async-done(((bf16[4,16,1024]{2,1,0:T(8,128)(2,1)}), bf16[4,16,1024]{2,1,0:T(8,128)(2,1)S(1)}, u32[]{:S(2)}, u32[]{:S(2)}) %all-to-all-start.1) | async-done | bytes 131104 | tf_op jit(solution)/shard_map/all_to_all | solution.py:470
  24.1 0.9 mix.1
  25.0 15.2 %all-to-all-start.2 = ((bf16[16,40,128]{2,1,0:T(8,128)(2,1)}), bf16[16,40,128]{2,1,0:T(8,128)(2,1)S(1)}, u32[]{:S(2)}, u32[]{:S(2)}) async-start(bf16[16,40,128]{2,1,0:T(8,128)(2,1)} %get-tuple-element.42), calls=%async_computation.2 | async-start | bytes 327680 | tf_op jit(solution)/shard_map/all_to_all | solution.py:492
  40.2 4.9 %collective-permute-start = (bf16[1,4,48,256]{3,2,1,0:T(8,128)(2,1)S(1)}, bf16[1,4,48,256]{3,2,1,0:T(8,128)(2,1)S(1)}, u32[]{:S(2)}, u32[]{:S(2)}) collective-permute-start(bf16[1,4,48,256]{3,2,1,0:T(8,128)(2,1)S(1)} %slice_bitcast_fusion), channel_id=1, source_target_pairs={{0,16},{4,20},{8,24},{12,28},{16,0},{20,4},{24,8},{28,12},{1,17},{... | collective-permute-start | bytes 294920 | tf_op jit(solution)/shard_map/ppermute | solution.py:378
  45.1 3.1 %collective-permute-done = bf16[1,4,48,256]{3,2,1,0:T(8,128)(2,1)S(1)} collective-permute-done((bf16[1,4,48,256]{3,2,1,0:T(8,128)(2,1)S(1)}, bf16[1,4,48,256]{3,2,1,0:T(8,128)(2,1)S(1)}, u32[]{:S(2)}, u32[]{:S(2)}) %collective-permute-start) | collective-permute-done | bytes 98336 | tf_op jit(solution)/shard_map/ppermute | solution.py:378
  48.2 3.4 %collective-permute-start.1 = (bf16[2,4,48,256]{3,2,1,0:T(8,128)(2,1)S(1)}, bf16[2,4,48,256]{3,2,1,0:T(8,128)(2,1)S(1)}, u32[]{:S(2)}, u32[]{:S(2)}) collective-permute-start(bf16[2,4,48,256]{3,2,1,0:T(8,128)(2,1)S(1)} %pad_maximum_fusion.1), channel_id=1, source_target_pairs={{0,8},{4,28},{8,0},{12,20},{16,24},{20,12},{24,16},{28,4},{1,9},{5... | collective-permute-start | bytes 589832 | tf_op jit(solution)/shard_map/ppermute | solution.py:378
  51.6 4.2 %collective-permute-done.1 = bf16[2,4,48,256]{3,2,1,0:T(8,128)(2,1)S(1)} collective-permute-done((bf16[2,4,48,256]{3,2,1,0:T(8,128)(2,1)S(1)}, bf16[2,4,48,256]{3,2,1,0:T(8,128)(2,1)S(1)}, u32[]{:S(2)}, u32[]{:S(2)}) %collective-permute-start.1) | collective-permute-done | bytes 196640 | tf_op jit(solution)/shard_map/ppermute | solution.py:378
  55.8 0.0 copy-start.1
  55.9 0.0 all-to-all-done.2.refs_1_
  55.9 1.4 %outward.1 = bf16[8,4,40,256]{3,2,1,0:T(8,128)(2,1)} custom-call(s32[1]{0:T(128)} %bitcast.11.refs_0_, bf16[16,40,128]{2,1,0:T(8,128)(2,1)S(1)} %all-to-all-done.2.refs_1_), custom_call_target="tpu_custom_call" | custom-call | tf_op jit(solution)/shard_map/outward/pallas_call | solution.py:499
  57.3 5.3 %all-to-all-start.3 = ((bf16[32,40,256]{2,1,0:T(8,128)(2,1)}), bf16[32,40,256]{2,1,0:T(8,128)(2,1)S(1)}, u32[]{:S(2)}, u32[]{:S(2)}) async-start(bf16[32,40,256]{2,1,0:T(8,128)(2,1)} %bitcast.22), calls=%async_computation.3 | async-start | bytes 1310720 | tf_op jit(solution)/shard_map/all_to_all | solution.py:512
  62.6 0.0 copy-done.1
  62.6 2.2 %collective-permute-start.2 = (bf16[4,4,48,256]{3,2,1,0:T(8,128)(2,1)S(1)}, bf16[4,4,48,256]{3,2,1,0:T(8,128)(2,1)S(1)}, u32[]{:S(2)}, u32[]{:S(2)}) collective-permute-start(bf16[4,4,48,256]{3,2,1,0:T(8,128)(2,1)S(1)} %pad_maximum_fusion.refs_3_), channel_id=1, source_target_pairs={{0,4},{4,0},{1,5},{5,1},{2,6},{6,2},{3,7},{7,3},{8,12},{12,8},{9,1... | collective-permute-start | bytes 1179656 | tf_op jit(solution)/shard_map/ppermute | solution.py:497
  64.8 1.4 %collective-permute-done.2.refs_4_ = bf16[4,4,48,256]{3,2,1,0:T(8,128)(2,1)S(1)} collective-permute-done((bf16[4,4,48,256]{3,2,1,0:T(8,128)(2,1)S(1)}, bf16[4,4,48,256]{3,2,1,0:T(8,128)(2,1)S(1)}, u32[]{:S(2)}, u32[]{:S(2)}) %collective-permute-start.2) | collective-permute-done | bytes 393248 | tf_op jit(solution)/shard_map/ppermute | solution.py:497
  66.2 0.0 copy-start.2
  66.2 0.8 copy-done.2
  67.0 1.6 %stage.3 = (bf16[1,1024,256]{2,1,0:T(8,128)(2,1)S(1)}, bf16[1,1024,256]{2,1,0:T(8,128)(2,1)S(1)}, bf16[1,256,1024]{2,1,0:T(8,128)(2,1)S(1)}, bf16[4,4,48,256]{3,...) custom-call(bf16[1,1024,256]{2,1,0:T(8,128)(2,1)} %refs_0_.1, bf16[1,1024,256]{2,1,0:T(8,128)(2,1)} %refs_1_.3, ...), custom_call_target="tpu_custom_call" | custom-call | tf_op jit(solution)/shard_map/stage/pallas_call | solution.py:114
  68.6 7.1 %all-to-all-done.3 = bf16[32,40,256]{2,1,0:T(8,128)(2,1)S(1)} async-done(((bf16[32,40,256]{2,1,0:T(8,128)(2,1)}), bf16[32,40,256]{2,1,0:T(8,128)(2,1)S(1)}, u32[]{:S(2)}, u32[]{:S(2)}) %all-to-all-start.3) | async-done | bytes 655392 | tf_op jit(solution)/shard_map/all_to_all | solution.py:512
  75.7 1.7 %experts.1 = bf16[8,4,40,256]{3,2,1,0:T(8,128)(2,1)} custom-call(bf16[8,4,40,256]{3,2,1,0:T(8,128)(2,1)S(1)} %bitcast.18, bf16[1,1024,256]{2,1,0:T(8,128)(2,1)S(1)} %get-tuple-element.45.refs_1_, bf16[1,1024,256]{2,1,0:T(8,128)(2,1)S(1)} %get-tuple-element.46.refs_2_, bf16[1,256,1024]{2,1,0:T(8,128)(2,1)S(1)} %get-tuple-element.47.refs_3_, ...), custom_call_target="tpu_custom_call" | custom-call | tf_op jit(solution)/shard_map/experts/pallas_call | solution.py:527
  77.4 3.9 %all-to-all-start.4 = ((bf16[32,40,256]{2,1,0:T(8,128)(2,1)}), bf16[32,40,256]{2,1,0:T(8,128)(2,1)S(1)}, u32[]{:S(2)}, u32[]{:S(2)}) async-start(bf16[32,40,256]{2,1,0:T(8,128)(2,1)} %bitcast.21), calls=%async_computation.4 | async-start | bytes 1310720 | tf_op jit(solution)/shard_map/all_to_all | solution.py:542
  81.3 0.9 weights.1
  82.1 12.2 %all-to-all-done.4 = bf16[32,40,256]{2,1,0:T(8,128)(2,1)S(1)} async-done(((bf16[32,40,256]{2,1,0:T(8,128)(2,1)}), bf16[32,40,256]{2,1,0:T(8,128)(2,1)S(1)}, u32[]{:S(2)}, u32[]{:S(2)}) %all-to-all-start.4) | async-done | bytes 655392 | tf_op jit(solution)/shard_map/all_to_all | solution.py:542
  94.4 0.3 inward.1
  94.6 25.4 %all_to_all.30 = bf16[16,16,256]{2,1,0:T(8,128)(2,1)S(1)} all-to-all(bf16[16,16,256]{2,1,0:T(8,128)(2,1)S(1)} %inward.1), channel_id=1, replica_groups=mesh['ep_0'=16,'ep_1'=4,'ep_2'=2,'tp'=4] {'ep_0'}, dimensions={0} | all-to-all | bytes 262144 | tf_op jit(solution)/shard_map/all_to_all | solution.py:551
  120.1 0.6 add_convert_fusion
  (4 shorter events, 0.1 us)
Async XLA Ops:
  2.1 10.5 %all-to-all-start = ((bf16[4,72,256]{2,1,0:T(8,128)(2,1)}), bf16[4,72,256]{2,1,0:T(8,128)(2,1)S(1)}, u32[]{:S(2)}, u32[]{:S(2)}) async-start(bf16[4,72,256]{2,1,0:T(8,128)(2,1)} %opening.1), calls=%async_computation | async-start | bytes 294912 | tf_op jit(solution)/shard_map/all_to_all | solution.py:435
  6.5 0.7 copy-start.4
  14.8 9.3 %all-to-all-start.1 = ((bf16[4,16,1024]{2,1,0:T(8,128)(2,1)}), bf16[4,16,1024]{2,1,0:T(8,128)(2,1)S(1)}, u32[]{:S(2)}, u32[]{:S(2)}) async-start(bf16[4,16,1024]{2,1,0:T(8,128)(2,1)} %get-tuple-element.39), calls=%async_computation.1 | async-start | bytes 262144 | tf_op jit(solution)/shard_map/all_to_all | solution.py:470
  18.2 0.7 copy-start
  18.9 0.7 copy-start.3
  25.0 30.9 %all-to-all-start.2 = ((bf16[16,40,128]{2,1,0:T(8,128)(2,1)}), bf16[16,40,128]{2,1,0:T(8,128)(2,1)S(1)}, u32[]{:S(2)}, u32[]{:S(2)}) async-start(bf16[16,40,128]{2,1,0:T(8,128)(2,1)} %get-tuple-element.42), calls=%async_computation.2 | async-start | bytes 327680 | tf_op jit(solution)/shard_map/all_to_all | solution.py:492
  40.2 8.0 %collective-permute-start = (bf16[1,4,48,256]{3,2,1,0:T(8,128)(2,1)S(1)}, bf16[1,4,48,256]{3,2,1,0:T(8,128)(2,1)S(1)}, u32[]{:S(2)}, u32[]{:S(2)}) collective-permute-start(bf16[1,4,48,256]{3,2,1,0:T(8,128)(2,1)S(1)} %slice_bitcast_fusion), channel_id=1, source_target_pairs={{0,16},{4,20},{8,24},{12,28},{16,0},{20,4},{24,8},{28,12},{1,17},{... | collective-permute-start | bytes 294920 | tf_op jit(solution)/shard_map/ppermute | solution.py:378
  48.2 7.6 %collective-permute-start.1 = (bf16[2,4,48,256]{3,2,1,0:T(8,128)(2,1)S(1)}, bf16[2,4,48,256]{3,2,1,0:T(8,128)(2,1)S(1)}, u32[]{:S(2)}, u32[]{:S(2)}) collective-permute-start(bf16[2,4,48,256]{3,2,1,0:T(8,128)(2,1)S(1)} %pad_maximum_fusion.1), channel_id=1, source_target_pairs={{0,8},{4,28},{8,0},{12,20},{16,24},{20,12},{24,16},{28,4},{1,9},{5... | collective-permute-start | bytes 589832 | tf_op jit(solution)/shard_map/ppermute | solution.py:378
  55.8 6.8 %copy-start.1 = (bf16[4,4,48,256]{3,2,1,0:T(8,128)(2,1)}, bf16[4,4,48,256]{3,2,1,0:T(8,128)(2,1)S(1)}, u32[]{:S(2)}) copy-start(bf16[4,4,48,256]{3,2,1,0:T(8,128)(2,1)S(1)} %pad_maximum_fusion.refs_3_) | copy-start | bytes 1179652
  57.3 18.4 %all-to-all-start.3 = ((bf16[32,40,256]{2,1,0:T(8,128)(2,1)}), bf16[32,40,256]{2,1,0:T(8,128)(2,1)S(1)}, u32[]{:S(2)}, u32[]{:S(2)}) async-start(bf16[32,40,256]{2,1,0:T(8,128)(2,1)} %bitcast.22), calls=%async_computation.3 | async-start | bytes 1310720 | tf_op jit(solution)/shard_map/all_to_all | solution.py:512
  62.6 3.6 %collective-permute-start.2 = (bf16[4,4,48,256]{3,2,1,0:T(8,128)(2,1)S(1)}, bf16[4,4,48,256]{3,2,1,0:T(8,128)(2,1)S(1)}, u32[]{:S(2)}, u32[]{:S(2)}) collective-permute-start(bf16[4,4,48,256]{3,2,1,0:T(8,128)(2,1)S(1)} %pad_maximum_fusion.refs_3_), channel_id=1, source_target_pairs={{0,4},{4,0},{1,5},{5,1},{2,6},{6,2},{3,7},{7,3},{8,12},{12,8},{9,1... | collective-permute-start | bytes 1179656 | tf_op jit(solution)/shard_map/ppermute | solution.py:497
  66.2 0.8 copy-start.2
  77.4 17.0 %all-to-all-start.4 = ((bf16[32,40,256]{2,1,0:T(8,128)(2,1)}), bf16[32,40,256]{2,1,0:T(8,128)(2,1)S(1)}, u32[]{:S(2)}, u32[]{:S(2)}) async-start(bf16[32,40,256]{2,1,0:T(8,128)(2,1)} %bitcast.21), calls=%async_computation.4 | async-start | bytes 1310720 | tf_op jit(solution)/shard_map/all_to_all | solution.py:542

commit v3 on v1

--- a/solution.py
+++ b/solution.py
@@ -121,6 +121,17 @@
     )(*map(far, arrays))
 
 
+def spread(message_ref, out_hbm, sems):
+    moves = [
+        pltpu.make_async_copy(message_ref, out_hbm.at[k], sems.at[k])
+        for k in range(out_hbm.shape[0])
+    ]
+    for move in moves:
+        move.start()
+    for move in moves:
+        move.wait()
+
+
 def attend_kernel(
     lambda_ref,
     pieces_ref,
@@ -135,9 +146,11 @@
     past_key_ref,
     past_value_ref,
     lengths_ref,
-    out_ref,
+    out_hbm,
     key_rows_ref,
     value_rows_ref,
+    part_ref,
+    sems,
 ):
     seq, past, size = past_key_ref.shape
     tp = pieces_ref.shape[0]
@@ -195,12 +208,11 @@
         mixed = mixed + mm(mine, past_value_ref[k])
     square = jnp.sum(mixed * mixed, axis=1, keepdims=True) / size
     head = mixed * lax.rsqrt(square + EPSILON) * sub_ref[...] * OUT_SCALE
-    part = mm(head.astype(jnp.bfloat16), out_weight_ref[...]).astype(jnp.bfloat16)
-    for k in range(tp):
-        out_ref[k] = part
-
-
-def mix_kernel(tp_ref, parts_ref, pieces_ref, gain_ref, routes_ref, res_ref, out_ref, *, top):
+    part_ref[...] = mm(head.astype(jnp.bfloat16), out_weight_ref[...]).astype(jnp.bfloat16)
+    spread(part_ref, out_hbm, sems)
+
+
+def mix_kernel(tp_ref, parts_ref, pieces_ref, gain_ref, routes_ref, res_ref, out_hbm, message_ref, sems, *, top):
     tp, seq, _ = parts_ref.shape
     past = pieces_ref.shape[1] - 8
     residual = jnp.concatenate([pieces_ref[k, :seq, :] for k in range(tp)], axis=1)
@@ -224,16 +236,16 @@
     lane = lax.broadcasted_iota(jnp.int32, routes.shape, 1)
     routes = jnp.where(lane == 3 * top, upper, routes)
     routes = jnp.where(lane == 3 * top + 1, branch - upper, routes)
-    rows = out_ref.shape[1] - width // LANES * seq
+    rows = message_ref.shape[0] - width // LANES * seq
     stride = LANES * rows // seq
     notes = routes[:rows]
     for g in range(1, seq // rows):
         notes = notes + pltpu.roll(routes[g * rows : (g + 1) * rows], stride * g, axis=1)
     notes = notes.astype(jnp.bfloat16)
-    for k in range(out_ref.shape[0]):
-        for h in range(width // LANES):
-            out_ref[k, h * seq : (h + 1) * seq, :] = mix[:, h * LANES : (h + 1) * LANES]
-        out_ref[k, width // LANES * seq :, :] = notes
+    for h in range(width // LANES):
+        message_ref[h * seq : (h + 1) * seq, :] = mix[:, h * LANES : (h + 1) * LANES]
+    message_ref[width // LANES * seq :, :] = notes
+    spread(message_ref, out_hbm, sems)
 
 
 def notes_of(seen_ref, seq):
@@ -449,11 +461,16 @@
     parts, key_rows, value_rows = pl.pallas_call(
         attend_kernel,
         out_shape=(
-            shaped((tp, seq, out_weight.shape[1]), jnp.bfloat16),
+            sent_to_hbm((tp, seq, out_weight.shape[1]), jnp.bfloat16),
             shaped((seq, size), jnp.bfloat16),
             shaped((seq, size), jnp.bfloat16),
         ),
         in_specs=[SCALARS] + [WHOLE] * 12,
+        out_specs=(pl.BlockSpec(memory_space=pl.ANY), WHOLE, WHOLE),
+        scratch_shapes=[
+            pltpu.VMEM((seq, out_weight.shape[1]), jnp.bfloat16),
+            pltpu.SemaphoreType.DMA((tp,)),
+        ],
         name="attend",
         compiler_params=LIMIT,
     )(
@@ -472,9 +489,14 @@
         lambda *refs: mix_kernel(*refs, top=top),
         out_shape=(
             shaped((seq, width), jnp.float32),
-            shaped((line, width // LANES * seq + 8, LANES), jnp.bfloat16),
+            sent_to_hbm((line, width // LANES * seq + 8, LANES), jnp.bfloat16),
         ),
         in_specs=[SCALARS] + [WHOLE] * 4,
+        out_specs=(WHOLE, pl.BlockSpec(memory_space=pl.ANY)),
+        scratch_shapes=[
+            pltpu.VMEM((width // LANES * seq + 8, LANES), jnp.bfloat16),
+            pltpu.SemaphoreType.DMA((line,)),
+        ],
         name="mix",
         compiler_params=LIMIT,
     )(

time: 122 us -> 122 us (level)
  no operation moved by 1% of the time
where the time goes in v3:
time: 122 us; the launch traced here: 121 us
  starting transfers between devices  42.8 us (35%)
  waiting for transfers between devices  34.7 us (28%)
  blocking collectives  25.4 us (21%)
  Pallas kernels  13.6 us (11%)
  local copies, waits for them, and re-layouts  2.96 us (2%)
  between operations  1.46 us (1%)
    all_to_all x1, blocking collectives, body(): home = lax.all_to_all(back, 'ep_0', 0, 0, tiled=True)  25.4 us
    all_to_all x1, starting transfers between devices, body(): seen = lax.all_to_all(message, 'ep_0', 0, 0, tiled=True)  15.2 us
    all_to_all x1, waiting for transfers between devices, body(): lax.all_to_all(sent.reshape(plane * tp, slots + dealt, width), BLOCK, 0,...  12.2 us
    ppermute x2, starting transfers between devices, doubled(): other = lax.ppermute(held, 'ep_1', [(i, i ^ step) for i in range(columns)])  8.33 us
    ppermute x2, waiting for transfers between devices, doubled(): other = lax.ppermute(held, 'ep_1', [(i, i ^ step) for i in range(columns)])  7.23 us
    all_to_all x1, waiting for transfers between devices, body(): lax.all_to_all(outward.reshape(plane * tp, slots + dealt, width), BLOCK,...  7.05 us
    all_to_all x1, starting transfers between devices, body(): lax.all_to_all(outward.reshape(plane * tp, slots + dealt, width), BLOCK,...  5.31 us
    all_to_all x1, starting transfers between devices, body(): pieces = lax.all_to_all(mine, 'tp', 0, 0, tiled=True)  4.46 us
  transfers between devices with their start and end apart: 8, of which 7 were waited for; matrix products, arithmetic and copies ran while one was open for 0% of the time, Pallas kernels for 4%

profile of v3, /device:TPU:32, one launch (start us, length us, event | category | flops | bytes accessed | tf_op | source)
XLA Modules:
  0.0 121.5 jit_solution(9224605141777412105)
XLA Ops:
  0.6 1.4 %opening.1 = bf16[4,72,256]{2,1,0:T(8,128)(2,1)} custom-call(bf16[16,256]{1,0:T(8,128)(2,1)} %hidden_ref.1, bf16[16,256]{1,0:T(8,128)(2,1)} %bitcast.23, bf16[16,256]{1,0:T(8,128)(2,1)} %bitcast.24, bf16[16,256]{1,0:T(8,128)(2,1)} %down_ref.1, f32[1,256]{1,0:T(1,128)} %bitcast.26, f32[1,256]{1,0:T(1,128)} %bitcast.28), custom_call_target="tpu_custom_call" | custom-call | tf_op jit(solution)/shard_map/opening/pallas_call | solution.py:427
  2.1 4.5 %all-to-all-start = ((bf16[4,72,256]{2,1,0:T(8,128)(2,1)}), bf16[4,72,256]{2,1,0:T(8,128)(2,1)S(1)}, u32[]{:S(2)}, u32[]{:S(2)}) async-start(bf16[4,72,256]{2,1,0:T(8,128)(2,1)} %opening.1), calls=%async_computation | async-start | bytes 294912 | tf_op jit(solution)/shard_map/all_to_all | solution.py:442
  6.5 0.0 copy-start.4
  6.5 0.7 copy-done.4
  7.2 0.1 copy.26.lengths_ref
  7.9 2.0 %stage.2 = (f32[1,1024]{1,0:T(1,128)S(1)}, bf16[1024,128]{1,0:T(8,128)(2,1)S(1)}, bf16[1024,128]{1,0:T(8,128)(2,1)S(1)}, bf16[1024,128]{1,0:T(8,128)(2,1)S(1)}, ...) custom-call(f32[1,1024]{1,0:T(1,128)} %bitcast.25, ...), custom_call_target="tpu_custom_call" | custom-call | tf_op jit(solution)/shard_map/stage/pallas_call | solution.py:113
  10.0 2.6 %all-to-all-done.pieces_ref.refs_2_ = bf16[4,72,256]{2,1,0:T(8,128)(2,1)S(1)} async-done(((bf16[4,72,256]{2,1,0:T(8,128)(2,1)}), bf16[4,72,256]{2,1,0:T(8,128)(2,1)S(1)}, u32[]{:S(2)}, u32[]{:S(2)}) %all-to-all-start) | async-done | bytes 147488 | tf_op jit(solution)/shard_map/all_to_all | solution.py:442
  12.6 2.9 %attend.1 = (bf16[4,16,1024]{2,1,0:T(8,128)(2,1)}, bf16[16,128]{1,0:T(8,128)(2,1)}, bf16[16,128]{1,0:T(8,128)(2,1)}) custom-call(f32[1]{0:T(128)S(6)} %copy.29.lambda_ref, bf16[4,72,256]{2,1,0:T(8,128)(2,1)S(1)} %all-to-all-done.pieces_ref.refs_2_, f32[1,1024]{1,0:T(1,128)S(1)} %get-tuple-element.29.gain_ref, ...), custom_call_target="tpu_custom_call" | custom-call | tf_op jit(solution)/shard_map/attend/pallas_call | solution.py:461
  15.5 3.3 %all-to-all-start.1 = ((bf16[4,16,1024]{2,1,0:T(8,128)(2,1)}), bf16[4,16,1024]{2,1,0:T(8,128)(2,1)S(1)}, u32[]{:S(2)}, u32[]{:S(2)}) async-start(bf16[4,16,1024]{2,1,0:T(8,128)(2,1)} %get-tuple-element.39), calls=%async_computation.1 | async-start | bytes 262144 | tf_op jit(solution)/shard_map/all_to_all | solution.py:482
  18.8 0.0 copy-start
  18.8 0.7 copy-done
  19.5 0.0 copy-start.3
  19.5 0.1 copy.27.ids_ref
  19.6 0.6 copy-done.3
  20.2 0.1 copy.28.logits_ref
  20.3 0.4 routes.1.refs_4_
  20.7 4.1 %all-to-all-done.1.refs_1_ = bf16[4,16,1024]{2,1,0:T(8,128)(2,1)S(1)} async-done(((bf16[4,16,1024]{2,1,0:T(8,128)(2,1)}), bf16[4,16,1024]{2,1,0:T(8,128)(2,1)S(1)}, u32[]{:S(2)}, u32[]{:S(2)}) %all-to-all-start.1) | async-done | bytes 131104 | tf_op jit(solution)/shard_map/all_to_all | solution.py:482
  24.8 1.0 mix.1
  25.8 15.2 %all-to-all-start.2 = ((bf16[16,40,128]{2,1,0:T(8,128)(2,1)}), bf16[16,40,128]{2,1,0:T(8,128)(2,1)S(1)}, u32[]{:S(2)}, u32[]{:S(2)}) async-start(bf16[16,40,128]{2,1,0:T(8,128)(2,1)} %get-tuple-element.42), calls=%async_computation.2 | async-start | bytes 327680 | tf_op jit(solution)/shard_map/all_to_all | solution.py:509
  41.0 4.9 %collective-permute-start = (bf16[1,4,48,256]{3,2,1,0:T(8,128)(2,1)S(1)}, bf16[1,4,48,256]{3,2,1,0:T(8,128)(2,1)S(1)}, u32[]{:S(2)}, u32[]{:S(2)}) collective-permute-start(bf16[1,4,48,256]{3,2,1,0:T(8,128)(2,1)S(1)} %slice_bitcast_fusion), channel_id=1, source_target_pairs={{0,16},{8,24},{16,0},{24,8},{1,17},{9,25},{17,1},{25,9},{2,18},{10... | collective-permute-start | bytes 294920 | tf_op jit(solution)/shard_map/ppermute | solution.py:385
  46.0 3.1 %collective-permute-done = bf16[1,4,48,256]{3,2,1,0:T(8,128)(2,1)S(1)} collective-permute-done((bf16[1,4,48,256]{3,2,1,0:T(8,128)(2,1)S(1)}, bf16[1,4,48,256]{3,2,1,0:T(8,128)(2,1)S(1)}, u32[]{:S(2)}, u32[]{:S(2)}) %collective-permute-start) | collective-permute-done | bytes 98336 | tf_op jit(solution)/shard_map/ppermute | solution.py:385
  49.1 3.4 %collective-permute-start.1 = (bf16[2,4,48,256]{3,2,1,0:T(8,128)(2,1)S(1)}, bf16[2,4,48,256]{3,2,1,0:T(8,128)(2,1)S(1)}, u32[]{:S(2)}, u32[]{:S(2)}) collective-permute-start(bf16[2,4,48,256]{3,2,1,0:T(8,128)(2,1)S(1)} %pad_maximum_fusion.1), channel_id=1, source_target_pairs={{0,8},{8,0},{16,24},{24,16},{1,9},{9,1},{17,25},{25,17},{2,10},{10... | collective-permute-start | bytes 589832 | tf_op jit(solution)/shard_map/ppermute | solution.py:385
  52.5 4.2 %collective-permute-done.1 = bf16[2,4,48,256]{3,2,1,0:T(8,128)(2,1)S(1)} collective-permute-done((bf16[2,4,48,256]{3,2,1,0:T(8,128)(2,1)S(1)}, bf16[2,4,48,256]{3,2,1,0:T(8,128)(2,1)S(1)}, u32[]{:S(2)}, u32[]{:S(2)}) %collective-permute-start.1) | collective-permute-done | bytes 196640 | tf_op jit(solution)/shard_map/ppermute | solution.py:385
  56.7 0.0 copy-start.1
  56.7 0.0 all-to-all-done.2.refs_1_
  56.7 1.4 %outward.1 = bf16[8,4,40,256]{3,2,1,0:T(8,128)(2,1)} custom-call(s32[1]{0:T(128)} %bitcast.11.refs_0_, bf16[16,40,128]{2,1,0:T(8,128)(2,1)S(1)} %all-to-all-done.2.refs_1_), custom_call_target="tpu_custom_call" | custom-call | tf_op jit(solution)/shard_map/outward/pallas_call | solution.py:516
  58.1 5.3 %all-to-all-start.3 = ((bf16[32,40,256]{2,1,0:T(8,128)(2,1)}), bf16[32,40,256]{2,1,0:T(8,128)(2,1)S(1)}, u32[]{:S(2)}, u32[]{:S(2)}) async-start(bf16[32,40,256]{2,1,0:T(8,128)(2,1)} %bitcast.22), calls=%async_computation.3 | async-start | bytes 1310720 | tf_op jit(solution)/shard_map/all_to_all | solution.py:529
  63.4 0.0 copy-done.1
  63.4 2.2 %collective-permute-start.2 = (bf16[4,4,48,256]{3,2,1,0:T(8,128)(2,1)S(1)}, bf16[4,4,48,256]{3,2,1,0:T(8,128)(2,1)S(1)}, u32[]{:S(2)}, u32[]{:S(2)}) collective-permute-start(bf16[4,4,48,256]{3,2,1,0:T(8,128)(2,1)S(1)} %pad_maximum_fusion.refs_3_), channel_id=1, source_target_pairs={{0,4},{4,0},{1,5},{5,1},{2,6},{6,2},{3,7},{7,3},{8,12},{12,8},{9,1... | collective-permute-start | bytes 1179656 | tf_op jit(solution)/shard_map/ppermute | solution.py:514
  65.6 1.4 %collective-permute-done.2.refs_4_ = bf16[4,4,48,256]{3,2,1,0:T(8,128)(2,1)S(1)} collective-permute-done((bf16[4,4,48,256]{3,2,1,0:T(8,128)(2,1)S(1)}, bf16[4,4,48,256]{3,2,1,0:T(8,128)(2,1)S(1)}, u32[]{:S(2)}, u32[]{:S(2)}) %collective-permute-start.2) | collective-permute-done | bytes 393248 | tf_op jit(solution)/shard_map/ppermute | solution.py:514
  67.1 0.0 copy-start.2
  67.1 0.8 copy-done.2
  67.8 1.6 %stage.3 = (bf16[1,1024,256]{2,1,0:T(8,128)(2,1)S(1)}, bf16[1,1024,256]{2,1,0:T(8,128)(2,1)S(1)}, bf16[1,256,1024]{2,1,0:T(8,128)(2,1)S(1)}, bf16[4,4,48,256]{3,...) custom-call(bf16[1,1024,256]{2,1,0:T(8,128)(2,1)} %refs_0_.1, bf16[1,1024,256]{2,1,0:T(8,128)(2,1)} %refs_1_.3, ...), custom_call_target="tpu_custom_call" | custom-call | tf_op jit(solution)/shard_map/stage/pallas_call | solution.py:113
  69.5 7.1 %all-to-all-done.3 = bf16[32,40,256]{2,1,0:T(8,128)(2,1)S(1)} async-done(((bf16[32,40,256]{2,1,0:T(8,128)(2,1)}), bf16[32,40,256]{2,1,0:T(8,128)(2,1)S(1)}, u32[]{:S(2)}, u32[]{:S(2)}) %all-to-all-start.3) | async-done | bytes 655392 | tf_op jit(solution)/shard_map/all_to_all | solution.py:529
  76.5 1.7 %experts.1 = bf16[8,4,40,256]{3,2,1,0:T(8,128)(2,1)} custom-call(bf16[8,4,40,256]{3,2,1,0:T(8,128)(2,1)S(1)} %bitcast.18, bf16[1,1024,256]{2,1,0:T(8,128)(2,1)S(1)} %get-tuple-element.45.refs_1_, bf16[1,1024,256]{2,1,0:T(8,128)(2,1)S(1)} %get-tuple-element.46.refs_2_, bf16[1,256,1024]{2,1,0:T(8,128)(2,1)S(1)} %get-tuple-element.47.refs_3_, ...), custom_call_target="tpu_custom_call" | custom-call | tf_op jit(solution)/shard_map/experts/pallas_call | solution.py:544
  78.2 3.9 %all-to-all-start.4 = ((bf16[32,40,256]{2,1,0:T(8,128)(2,1)}), bf16[32,40,256]{2,1,0:T(8,128)(2,1)S(1)}, u32[]{:S(2)}, u32[]{:S(2)}) async-start(bf16[32,40,256]{2,1,0:T(8,128)(2,1)} %bitcast.21), calls=%async_computation.4 | async-start | bytes 1310720 | tf_op jit(solution)/shard_map/all_to_all | solution.py:559
  82.1 0.9 weights.1
  83.0 12.2 %all-to-all-done.4 = bf16[32,40,256]{2,1,0:T(8,128)(2,1)S(1)} async-done(((bf16[32,40,256]{2,1,0:T(8,128)(2,1)}), bf16[32,40,256]{2,1,0:T(8,128)(2,1)S(1)}, u32[]{:S(2)}, u32[]{:S(2)}) %all-to-all-start.4) | async-done | bytes 655392 | tf_op jit(solution)/shard_map/all_to_all | solution.py:559
  95.2 0.3 inward.1
  95.4 25.4 %all_to_all.30 = bf16[16,16,256]{2,1,0:T(8,128)(2,1)S(1)} all-to-all(bf16[16,16,256]{2,1,0:T(8,128)(2,1)S(1)} %inward.1), channel_id=1, replica_groups=mesh['ep_0'=16,'ep_1'=4,'ep_2'=2,'tp'=4] {'ep_0'}, dimensions={0} | all-to-all | bytes 262144 | tf_op jit(solution)/shard_map/all_to_all | solution.py:568
  120.9 0.6 add_convert_fusion
  (4 shorter events, 0.1 us)
Async XLA Ops:
  2.1 10.5 %all-to-all-start = ((bf16[4,72,256]{2,1,0:T(8,128)(2,1)}), bf16[4,72,256]{2,1,0:T(8,128)(2,1)S(1)}, u32[]{:S(2)}, u32[]{:S(2)}) async-start(bf16[4,72,256]{2,1,0:T(8,128)(2,1)} %opening.1), calls=%async_computation | async-start | bytes 294912 | tf_op jit(solution)/shard_map/all_to_all | solution.py:442
  6.5 0.7 copy-start.4
  15.5 9.3 %all-to-all-start.1 = ((bf16[4,16,1024]{2,1,0:T(8,128)(2,1)}), bf16[4,16,1024]{2,1,0:T(8,128)(2,1)S(1)}, u32[]{:S(2)}, u32[]{:S(2)}) async-start(bf16[4,16,1024]{2,1,0:T(8,128)(2,1)} %get-tuple-element.39), calls=%async_computation.1 | async-start | bytes 262144 | tf_op jit(solution)/shard_map/all_to_all | solution.py:482
  18.8 0.7 copy-start
  19.5 0.7 copy-start.3
  25.8 30.9 %all-to-all-start.2 = ((bf16[16,40,128]{2,1,0:T(8,128)(2,1)}), bf16[16,40,128]{2,1,0:T(8,128)(2,1)S(1)}, u32[]{:S(2)}, u32[]{:S(2)}) async-start(bf16[16,40,128]{2,1,0:T(8,128)(2,1)} %get-tuple-element.42), calls=%async_computation.2 | async-start | bytes 327680 | tf_op jit(solution)/shard_map/all_to_all | solution.py:509
  41.0 8.0 %collective-permute-start = (bf16[1,4,48,256]{3,2,1,0:T(8,128)(2,1)S(1)}, bf16[1,4,48,256]{3,2,1,0:T(8,128)(2,1)S(1)}, u32[]{:S(2)}, u32[]{:S(2)}) collective-permute-start(bf16[1,4,48,256]{3,2,1,0:T(8,128)(2,1)S(1)} %slice_bitcast_fusion), channel_id=1, source_target_pairs={{0,16},{8,24},{16,0},{24,8},{1,17},{9,25},{17,1},{25,9},{2,18},{10... | collective-permute-start | bytes 294920 | tf_op jit(solution)/shard_map/ppermute | solution.py:385
  49.1 7.6 %collective-permute-start.1 = (bf16[2,4,48,256]{3,2,1,0:T(8,128)(2,1)S(1)}, bf16[2,4,48,256]{3,2,1,0:T(8,128)(2,1)S(1)}, u32[]{:S(2)}, u32[]{:S(2)}) collective-permute-start(bf16[2,4,48,256]{3,2,1,0:T(8,128)(2,1)S(1)} %pad_maximum_fusion.1), channel_id=1, source_target_pairs={{0,8},{8,0},{16,24},{24,16},{1,9},{9,1},{17,25},{25,17},{2,10},{10... | collective-permute-start | bytes 589832 | tf_op jit(solution)/shard_map/ppermute | solution.py:385
  56.7 6.8 %copy-start.1 = (bf16[4,4,48,256]{3,2,1,0:T(8,128)(2,1)}, bf16[4,4,48,256]{3,2,1,0:T(8,128)(2,1)S(1)}, u32[]{:S(2)}) copy-start(bf16[4,4,48,256]{3,2,1,0:T(8,128)(2,1)S(1)} %pad_maximum_fusion.refs_3_) | copy-start | bytes 1179652
  58.1 18.4 %all-to-all-start.3 = ((bf16[32,40,256]{2,1,0:T(8,128)(2,1)}), bf16[32,40,256]{2,1,0:T(8,128)(2,1)S(1)}, u32[]{:S(2)}, u32[]{:S(2)}) async-start(bf16[32,40,256]{2,1,0:T(8,128)(2,1)} %bitcast.22), calls=%async_computation.3 | async-start | bytes 1310720 | tf_op jit(solution)/shard_map/all_to_all | solution.py:529
  63.4 3.6 %collective-permute-start.2 = (bf16[4,4,48,256]{3,2,1,0:T(8,128)(2,1)S(1)}, bf16[4,4,48,256]{3,2,1,0:T(8,128)(2,1)S(1)}, u32[]{:S(2)}, u32[]{:S(2)}) collective-permute-start(bf16[4,4,48,256]{3,2,1,0:T(8,128)(2,1)S(1)} %pad_maximum_fusion.refs_3_), channel_id=1, source_target_pairs={{0,4},{4,0},{1,5},{5,1},{2,6},{6,2},{3,7},{7,3},{8,12},{12,8},{9,1... | collective-permute-start | bytes 1179656 | tf_op jit(solution)/shard_map/ppermute | solution.py:514
  67.1 0.8 copy-start.2
  78.2 17.0 %all-to-all-start.4 = ((bf16[32,40,256]{2,1,0:T(8,128)(2,1)}), bf16[32,40,256]{2,1,0:T(8,128)(2,1)S(1)}, u32[]{:S(2)}, u32[]{:S(2)}) async-start(bf16[32,40,256]{2,1,0:T(8,128)(2,1)} %bitcast.21), calls=%async_computation.4 | async-start | bytes 1310720 | tf_op jit(solution)/shard_map/all_to_all | solution.py:559
